TPU v7x, 32 devices: a whole 2x2x4 slice. The times are simulated.
32 devices in a mesh: sp: 4 (over y, x), tp: 8 (over z, core).
Axes of the slice: x: 2, y: 2, z: 4, core: 2. Of those that a mesh axis runs over, the one named last changes fastest.
Arguments:
- residual: bfloat16 [1536, 2048], P(('sp', 'tp')), may hold values from -40 to 40
- queries: bfloat16 [1536, 16, 256], P('sp', 'tp'), may hold values from -8.8 to 8.8
- query_rope: bfloat16 [1536, 16, 64], P('sp', 'tp'), may hold values from -72 to 72
- latent: bfloat16 [1536, 512], P('sp'), may hold values from -320 to 320
- key_rope: bfloat16 [1536, 32], P('sp'), may hold values from -48 to 48
- latent_gain: float32 [512], replicated, may hold values from 0.1 to 1.9
- key_weight: bfloat16 [512, 16, 256], P(None, 'tp'), may hold values from -0.25 to 0.25
- value_weight: bfloat16 [512, 16, 256], P(None, 'tp'), may hold values from -0.25 to 0.25
- out_weight: bfloat16 [16, 256, 2048], P('tp'), may hold values from -0.09375 to 0.09375
- norm_gain: float32 [2048], replicated, may hold values from 0.1 to 1.9
- routes: int32 [1536, 2], P('sp'), may hold values from 0 to 7, as said below
- group_gate: float32 [1536], P(('sp', 'tp')), may hold values from 0.5 to 1
- expert_share: float32 [1536, 2], P(('sp', 'tp')), may hold values from 0.2 to 1
- gate_weight: bfloat16 [8, 2048, 4096], P('sp', None, 'tp'), may hold values from -0.125 to 0.125
- up_weight: bfloat16 [8, 2048, 4096], P('sp', None, 'tp'), may hold values from -0.125 to 0.125
- down_weight: bfloat16 [8, 4096, 2048], P('sp', 'tp'), may hold values from -0.1875 to 0.1875
Outputs:
- layer_out: bfloat16 [1536, 2048], P(('sp', 'tp'))
Inputs may be any that keep to these rules, and one draw needn't show every extreme that they name: `routes`: each token names two different experts of one group; expert e belongs to group e // 2. In each aligned block of 48 tokens no expert is named more than 18 times, and one expert, the same in every block, is named exactly 18 times in every block.
All inputs are finite; a program needn't handle non-finite values.
Results may differ from a plain program's by a relative error of at most 0.025.
Values may be sent and summed in bfloat16 or wider, within the bound.
A program may use at most 64 MiB of HBM per device.

v0:
```python
import jax
import jax.numpy as jnp
from jax import lax
from jax.sharding import PartitionSpec as P

DK_A = 64
DV_A = 64


rope_base = 10000.0
epsilon = 1e-06
floor_score = -1e30


def angle_tables(places, rope_width):
    frequencies = rope_base ** (-jnp.arange(0, rope_width, 2, dtype=jnp.float32) / rope_width)
    angles = places[:, None] * frequencies[None, :]
    return (jnp.cos(angles), jnp.sin(angles))


def rope_turn(values, cosine, sine_table):
    half_size = values.shape[-1] // 2
    first_half = values[..., :half_size]
    second = values[..., half_size:]
    return jnp.concatenate(
        [first_half * cosine - second * sine_table, second * cosine + first_half * sine_table],
        axis=-1,
    )


def rms_scale(values, gain_vector):
    values = values.astype(jnp.float32)
    inverse = lax.rsqrt(jnp.mean(values * values, axis=-1, keepdims=True) + epsilon)
    return values * inverse * gain_vector


def online_step(
    carried, query_nope, query_turned, key_nope, piece_rope, value_part, visible, scale
):
    row_top, weight_sum, accumulated = carried
    scores = jnp.einsum("qhd,khd->hqk", query_nope, key_nope, preferred_element_type=jnp.float32)
    scores = scores + jnp.einsum(
        "qhd,kd->hqk", query_turned, piece_rope, preferred_element_type=jnp.float32
    )
    scores = scores * scale
    masked = jnp.where(visible[None], scores, floor_score)
    new_top = jnp.maximum(row_top, jnp.max(masked, axis=2))
    weights = jnp.where(visible[None], jnp.exp(masked - new_top[:, :, None]), 0.0)
    factor = jnp.exp(row_top - new_top)
    weight_sum = weight_sum * factor + jnp.sum(weights, axis=2)
    update = jnp.einsum(
        "hqk,khd->qhd", weights.astype(jnp.bfloat16), value_part, preferred_element_type=jnp.float32
    )
    accumulated = accumulated * jnp.transpose(factor)[:, :, None] + update
    return (new_top, weight_sum, accumulated)


def slot_table(route_block, experts_all, capacity):
    flat_routes = route_block.reshape(-1)
    onehot = (flat_routes[:, None] == jnp.arange(experts_all, dtype=jnp.int32)[None, :]).astype(
        jnp.int32
    )
    rank_within = jnp.sum((jnp.cumsum(onehot, axis=0) - onehot) * onehot, axis=1)
    return flat_routes * capacity + rank_within


def local(
    residual,
    queries,
    query_rope,
    latent,
    key_rope,
    latent_gain,
    key_weight,
    value_weight,
    out_weight,
    norm_gain,
    routes,
    group_gate,
    expert_share,
    gate_weight,
    up_weight,
    down_weight,
):
    local_tokens = queries.shape[0]
    pair_dev = queries.shape[1]
    sp_count = lax.axis_size("sp")
    tp_count = lax.axis_size("tp")
    row_count = local_tokens // tp_count
    rope_width = key_rope.shape[1]
    first_place = lax.axis_index("sp") * local_tokens
    places = (first_place + jnp.arange(local_tokens, dtype=jnp.int32)).astype(jnp.float32)
    cosine, sine_table = angle_tables(places, rope_width)
    rotated_key = rope_turn(key_rope.astype(jnp.float32), cosine, sine_table).astype(jnp.bfloat16)
    turned = rope_turn(
        query_rope.astype(jnp.float32).reshape(local_tokens, pair_dev, 2, rope_width),
        cosine[:, None, None, :],
        sine_table[:, None, None, :],
    ).astype(jnp.bfloat16)
    compressed = rms_scale(latent, latent_gain).astype(jnp.bfloat16)
    scale_one = (DK_A + rope_width) ** (-0.5)
    scale_two = (queries.shape[2] - DK_A + rope_width) ** (-0.5)
    key_flat = key_weight.reshape(key_weight.shape[0], -1)
    value_flat = value_weight.reshape(value_weight.shape[0], -1)

    def attend_piece(carried, piece_keys, piece_values, piece_rope, piece_start):
        key_count = piece_keys.shape[0]
        key_places = (piece_start + jnp.arange(key_count, dtype=jnp.int32)).astype(jnp.float32)
        visible = places[:, None] >= key_places[None, :]
        state_one = online_step(
            carried[0],
            queries[:, :, :DK_A],
            turned[:, :, 0],
            piece_keys[:, :, :DK_A],
            piece_rope,
            piece_values[:, :, :DV_A],
            visible,
            scale_one,
        )
        state_two = online_step(
            carried[1],
            queries[:, :, DK_A:],
            turned[:, :, 1],
            piece_keys[:, :, DK_A:],
            piece_rope,
            piece_values[:, :, DV_A:],
            visible,
            scale_two,
        )
        return (state_one, state_two)

    def empty_state(value_size):
        return (
            jnp.full((pair_dev, local_tokens), floor_score, jnp.float32),
            jnp.zeros((pair_dev, local_tokens), jnp.float32),
            jnp.zeros((local_tokens, pair_dev, value_size), jnp.float32),
        )

    initial = (empty_state(DV_A), empty_state(value_weight.shape[2] - DV_A))
    own_keys = (
        jnp.dot(compressed, key_flat, preferred_element_type=jnp.float32)
        .astype(jnp.bfloat16)
        .reshape(local_tokens, pair_dev, -1)
    )
    own_values = (
        jnp.dot(compressed, value_flat, preferred_element_type=jnp.float32)
        .astype(jnp.bfloat16)
        .reshape(local_tokens, pair_dev, -1)
    )

    def projected_step(carried, sub_pieces, block_start):
        return attend_piece(carried, sub_pieces[0], sub_pieces[1], sub_pieces[2], block_start)

    carried = initial
    pieces = (
        lax.all_gather(own_keys, "sp", axis=0, tiled=True),
        lax.all_gather(own_values, "sp", axis=0, tiled=True),
        lax.all_gather(rotated_key, "sp", axis=0, tiled=True),
    )
    key_count = pieces[0].shape[0]
    blocks = key_count // local_tokens
    block_size = key_count // blocks

    def one_block(running, block_index):
        block_start = block_index * block_size
        sub_pieces = tuple(
            (
                lax.dynamic_slice_in_dim(member, block_index * block_size, block_size, 0)
                for member in pieces
            )
        )

        def compute(running_state):
            return projected_step(running_state, sub_pieces, block_start)

        def keep_state(running_state):
            return running_state

        return (
            lax.cond(block_start < first_place + local_tokens, compute, keep_state, running),
            None,
        )

    carried, unused = lax.scan(one_block, carried, jnp.arange(blocks, dtype=jnp.int32))
    part_one = carried[0][2] / jnp.transpose(carried[0][1])[:, :, None]
    part_two = carried[1][2] / jnp.transpose(carried[1][1])[:, :, None]
    attention = (
        jnp.concatenate([part_one, part_two], axis=2).astype(jnp.bfloat16).reshape(local_tokens, -1)
    )
    out_flat = out_weight.reshape(-1, out_weight.shape[2])
    head_total = lax.psum_scatter(
        jnp.dot(attention, out_flat, preferred_element_type=jnp.float32).astype(jnp.bfloat16),
        "tp",
        scatter_dimension=0,
        tiled=True,
    ).astype(jnp.float32)
    mixed_rows = residual.astype(jnp.float32) + head_total
    normed = rms_scale(mixed_rows, norm_gain).astype(jnp.bfloat16)
    experts_dev = gate_weight.shape[0]
    experts_all = experts_dev * sp_count
    top_count = routes.shape[1]
    capacity = max(2, 3 * row_count * top_count // (2 * experts_all))
    slot_count = experts_all * capacity
    own_routes = lax.dynamic_slice_in_dim(routes, lax.axis_index("tp") * row_count, row_count, 0)
    own_slots = slot_table(own_routes, experts_all, capacity)
    pick_matrix = (jnp.arange(slot_count, dtype=jnp.int32)[:, None] == own_slots[None, :]).astype(
        jnp.bfloat16
    )
    pick_matrix = pick_matrix.reshape(slot_count, row_count, top_count).sum(axis=2)
    outgoing = (
        jnp.dot(pick_matrix, normed, preferred_element_type=jnp.float32)
        .astype(jnp.bfloat16)
        .reshape(sp_count, experts_dev, capacity, -1)
    )
    arrived = lax.all_to_all(outgoing, "sp", split_axis=0, concat_axis=0, tiled=True)
    gathered = lax.all_gather(arrived, "tp", axis=0, tiled=True)
    gate_out = jnp.einsum(
        "secd,edf->secf", gathered, gate_weight, preferred_element_type=jnp.float32
    )
    up_out = jnp.einsum("secd,edf->secf", gathered, up_weight, preferred_element_type=jnp.float32)
    hidden = (jax.nn.silu(gate_out) * up_out).astype(jnp.bfloat16)
    expert_out = lax.psum_scatter(
        jnp.einsum(
            "secf,efd->secd", hidden, down_weight, preferred_element_type=jnp.float32
        ).astype(jnp.bfloat16),
        "tp",
        scatter_dimension=0,
        tiled=True,
    )
    returned = lax.all_to_all(expert_out, "sp", split_axis=0, concat_axis=0, tiled=True).reshape(
        slot_count, -1
    )
    selectors = (own_slots[:, None] == jnp.arange(slot_count, dtype=jnp.int32)[None, :]).astype(
        jnp.bfloat16
    )
    picked = jnp.dot(selectors, returned, preferred_element_type=jnp.float32).reshape(
        row_count, top_count, -1
    )
    route_weight = group_gate[:, None] * expert_share / jnp.sum(expert_share, axis=1, keepdims=True)
    expert_mix = jnp.sum(route_weight[:, :, None] * picked, axis=1)
    return (mixed_rows + expert_mix).astype(jnp.bfloat16)


def solution(mesh):
    return jax.shard_map(
        local,
        mesh=mesh,
        in_specs=(
            P(("sp", "tp"), None),
            P("sp", "tp", None),
            P("sp", "tp", None),
            P("sp", None),
            P("sp", None),
            P(),
            P(None, "tp", None),
            P(None, "tp", None),
            P("tp", None, None),
            P(),
            P("sp", None),
            P(("sp", "tp")),
            P(("sp", "tp"), None),
            P("sp", None, "tp"),
            P("sp", None, "tp"),
            P("sp", "tp", None),
        ),
        out_specs=P(("sp", "tp"), None),
        check_vma=False,
    )
```

profile of v0, /device:TPU:0, one launch (start us, length us, event | category | flops | bytes accessed | tf_op | source)
XLA Modules:
  0.0 374.4 jit_solution(7903477350148555933)
XLA Ops:
  6.5 1.3 fusion.70
  7.9 1.1 copy.108
  9.0 1.5 convolution_convert_fusion.2
  10.5 0.9 copy.104
  12.1 0.9 copy.105
  13.5 0.7 copy.88
  14.2 9.9 %all_gather.13 = bf16[1536,32]{0,1:T(8,128)(2,1)S(1)} all-gather(bf16[384,32]{0,1:T(8,128)(2,1)S(1)} %pad_maximum_fusion.1), channel_id=1, replica_groups=mesh['sp'=4,'tp'=8] {'sp'}, dimensions={0}, use_global_device_ids=true | all-gather | bytes 122880 | tf_op jit(solution)/shard_map/all_gather | solution.py:158
  24.1 20.9 %all-gather.4.cloned.1.call-done = bf16[1536,2,256]{0,2,1:T(8,128)(2,1)} async-done(((bf16[384,2,256]{0,2,1:T(8,128)(2,1)}), bf16[1536,2,256]{0,2,1:T(8,128)(2,1)}) %all-gather.4.cloned.1.call-update) | async-done | bytes 1572880 | tf_op jit(solution)/shard_map/all_gather | solution.py:156
  45.1 32.6 %all-gather.6.cloned.1.call-done = bf16[1536,2,256]{0,2,1:T(8,128)(2,1)} async-done(((bf16[384,2,256]{0,2,1:T(8,128)(2,1)}), bf16[1536,2,256]{0,2,1:T(8,128)(2,1)}) %all-gather.6.cloned.1.call-update) | async-done | bytes 1572880 | tf_op jit(solution)/shard_map/all_gather | solution.py:157
  77.7 13.4 %while.23 = (s32[]{:T(128)}, f32[2,384]{1,0:T(2,128)S(1)}, f32[2,384]{1,0:T(2,128)S(1)}, f32[384,2,64]{0,2,1:T(8,128)S(1)}, f32[2,384]{1,0:T(2,128)S(1)}, /*inde...) while((s32[]{:T(128)}, f32[2,384]{1,0:T(2,128)S(1)}, ...), condition=%wide.region_8.9_spmd.clone, body=%wide.region_1.8_spmd.clone.sunk | while | flops 346183680 | bytes 15686121 | solution.py:184
  77.8 0.6 dynamic_slice.57
  79.1 7.9 %conditional.3 = ((f32[2,384]{1,0:T(2,128)S(1)}, f32[2,384]{1,0:T(2,128)S(1)}, f32[384,2,64]{0,2,1:T(8,128)S(1)}, f32[2,384]{1,0:T(2,128)S(1)}, f32[2,384]{1,0:T(2,128)S(1)}, /*index=5*/f32[384,2,192]{0,2,1:T(8,128)S(1)})) conditional(s32[]{:T(128)} %convert_element_type.168, (f32[2,384]{1,0:T(2,128)S(1)}, f32[2,384]{1,0:T(2,128)S(1)}, ...), branch_computations={%region_2.2_spmd, %region_3.7_spmd} | conditional | flops 346182912 | bytes 15684234 | solution.py:180
  79.1 1.7 convolution_bitcast_fusion.3
  81.6 1.7 fusion.8
  83.3 1.4 convolution_bitcast_fusion.2
  85.2 1.4 fusion.9
  91.2 0.9 copy.90
  92.4 1.2 divide_convert_fusion.1
  93.8 2.2 bitcast_convert_fusion
  97.7 56.2 %reduce-scatter.3.cloned.1.call-done = bf16[48,2048]{1,0:T(8,128)(2,1)} async-done(((bf16[384,2048]{1,0:T(8,128)(2,1)}), bf16[48,2048]{1,0:T(8,128)(2,1)}) %reduce-scatter.3.cloned.1.call-update) | async-done | bytes 196624 | tf_op jit(solution)/shard_map/reduce_scatter | solution.py:191
  153.9 1.1 multiply_reduce_fusion
  155.1 1.3 convolution_convert_fusion
  157.1 11.4 %all_to_all.10 = bf16[4,2,18,2048]{3,1,2,0:T(2,128)(2,1)} all-to-all(bf16[4,2,18,2048]{3,1,2,0:T(2,128)(2,1)S(1)} %copy.94), channel_id=1, replica_groups=mesh['sp'=4,'tp'=8] {'sp'}, dimensions={0} | all-to-all | bytes 1179648 | tf_op jit(solution)/shard_map/all_to_all | solution.py:215
  168.8 49.7 %all-gather.8.cloned.1.call-done = bf16[32,2,18,2048]{3,1,2,0:T(2,128)(2,1)} async-done(((bf16[4,2,18,2048]{3,1,2,0:T(2,128)(2,1)}), bf16[32,2,18,2048]{3,1,2,0:T(2,128)(2,1)}) %all-gather.8.cloned.1.call-update) | async-done | bytes 4718608 | tf_op jit(solution)/shard_map/all_gather | solution.py:216
  218.5 10.3 %fusion.50 = f32[2,32,18,512]{3,1,2,0:T(8,128)} fusion(bf16[2,2048,512]{2,1,0:T(8,128)(2,1)} %param.33, bf16[32,2,18,2048]{3,1,2,0:T(2,128)(2,1)} %all-gather.8.cloned.1.call-done), kind=kOutput, calls=%fused_computation.63 | convolution fusion | flops 2415919104 | bytes 11272192 | tf_op jit(solution)/shard_map/secd,edf->secf/dot_general | solution.py:217
  228.9 16.0 %convert_bitcast_fusion = bf16[32,2,18,2048]{3,0,2,1:T(8,128)(2,1)} fusion(bf16[2,512,2048]{2,1,0:T(8,128)(2,1)} %param.35, f32[2,32,18,512]{3,1,2,0:T(8,128)} %fusion.50, bf16[2,2048,512]{2,1,0:T(8,128)(2,1)} %param.34, bf16[32,2,18,2048]{3,1,2,0:T(2,128)(2,1)} %all-gather.8.cloned.1.call-done), kind=kOutput, calls=%fused_computation.58 | convolution fusion | flops 4837736448 | bytes 20185088 | tf_op jit(solution)/shard_map/secf,efd->secd/dot_general | solution.py:223
  246.7 103.4 %all-reduce.3.cloned.1.call-done = bf16[32,2,18,2048]{3,0,2,1:T(8,128)(2,1)} async-done(((bf16[32,2,18,2048]{3,0,2,1:T(8,128)(2,1)}), bf16[32,2,18,2048]{3,0,2,1:T(8,128)(2,1)}) %all-reduce.3.cloned.1.call-update) | async-done | bytes 4718608
  350.1 1.6 constant_dynamic-slice_fusion
  351.8 1.4 copy.97
  353.2 3.6 all-to-all-start.1
  356.9 8.5 %all-to-all-done.1 = bf16[4,2,18,2048]{3,1,2,0:T(2,128)(2,1)S(1)} async-done(((bf16[4,2,18,2048]{3,1,2,0:T(2,128)(2,1)}), bf16[4,2,18,2048]{3,1,2,0:T(2,128)(2,1)S(1)}, u32[]{:S(2)}, u32[]{:S(2)}) %all-to-all-start.1) | async-done | bytes 589856 | tf_op jit(solution)/shard_map/all_to_all | solution.py:230
  366.1 1.8 add_convert_fusion.2
  (96 shorter events, 9.9 us)
Async XLA Ops:
  6.5 87.2 %copy-start = (bf16[2,256,2048]{2,1,0:T(8,128)(2,1)S(1)}, bf16[2,256,2048]{2,1,0:T(8,128)(2,1)}, u32[]{:S(2)}) copy-start(bf16[2,256,2048]{2,1,0:T(8,128)(2,1)} %param.28) | copy-start | bytes 6291460
  6.5 38.5 %all-gather.4.cloned.1.call-start = ((), (), s32[]{:S(2)}) async-start(), calls=%async_computation.3 | async-start | bytes 1966080 | tf_op jit(solution)/shard_map/all_gather | solution.py:156
  9.0 2.6 copy-start.2
  9.0 2.7 copy-start.3
  9.0 2.7 copy-start.11
  11.5 66.1 %all-gather.6.cloned.1.call-start = ((), (), s32[]{:S(2)}) async-start(), calls=%async_computation.4 | async-start | bytes 1966080 | tf_op jit(solution)/shard_map/all_gather | solution.py:157
  11.6 1.5 copy-start.6
  11.7 1.5 copy-start.5
  12.1 1.4 copy-start.4
  13.1 140.9 %reduce-scatter.3.cloned.1.call-start = ((), (), s32[]{:S(2)}) async-start(), calls=%async_computation.5 | async-start | bytes 1769472 | tf_op jit(solution)/shard_map/reduce_scatter | solution.py:191
  96.0 0.7 copy-start.9
  96.0 58.0 %copy-start.1 = (bf16[48,2048]{1,0:T(8,128)(2,1)S(1)}, bf16[48,2048]{1,0:T(8,128)(2,1)}, u32[]{:S(2)}) copy-start(bf16[48,2048]{1,0:T(8,128)(2,1)} %param.20) | copy-start | bytes 589828
  96.0 59.1 %copy-start.7 = (f32[2048]{0:T(1024)S(1)}, f32[2048]{0:T(1024)}, u32[]{:S(2)}) copy-start(f32[2048]{0:T(1024)} %param.29) | copy-start | bytes 24580
  96.0 122.6 %all-gather.8.cloned.1.call-start = ((), (), s32[]{:S(2)}) async-start(), calls=%async_computation.6 | async-start | bytes 5308416 | tf_op jit(solution)/shard_map/all_gather | solution.py:216
  168.6 181.5 %all-reduce.3.cloned.1.call-start = ((), (), s32[]{:S(2)}) async-start(), calls=%async_computation.7 | async-start | bytes 9437184
  244.8 0.7 copy-start.12
  246.7 110.1 %copy-start.8 = (f32[48,2]{0,1:T(2,128)S(1)}, f32[48,2]{0,1:T(2,128)}, u32[]{:S(2)}) copy-start(f32[48,2]{0,1:T(2,128)} %param.32) | copy-start | bytes 1156
  246.7 110.1 %copy-start.10 = (f32[48]{0:T(128)S(1)}, f32[48]{0:T(128)}, u32[]{:S(2)}) copy-start(f32[48]{0:T(128)} %param.31) | copy-start | bytes 580
  353.2 12.2 %all-to-all-start.1 = ((bf16[4,2,18,2048]{3,1,2,0:T(2,128)(2,1)}), bf16[4,2,18,2048]{3,1,2,0:T(2,128)(2,1)S(1)}, u32[]{:S(2)}, u32[]{:S(2)}) async-start(bf16[4,2,18,2048]{3,1,2,0:T(2,128)(2,1)} %copy.97), calls=%async_computation.2 | async-start | bytes 1179648 | tf_op jit(solution)/shard_map/all_to_all | solution.py:230
Sparse Core Ops, SparseCore 0:
  11.6 33.4 all-gather.3
  46.9 30.6 all-gather.5
  96.1 57.7 reduce-scatter.2
  168.7 49.7 all-gather.7
  245.0 105.1 all-reduce.2
where the time goes:
time: 375 us; the launch traced here: 374 us
  waiting for transfers between devices  271 us (72%)
  matrix products  39.2 us (10%)
  blocking collectives  21.4 us (6%)
  local copies, waits for them, and re-layouts  14.2 us (4%)
  between operations  14.2 us (4%)
  other arithmetic  7.03 us (2%)
  starting transfers between devices  4 us (1%)
    unnamed x6, waiting for transfers between devices  103 us
    reduce_scatter x1, waiting for transfers between devices, local(): lax.psum_scatter(jnp.dot(attention, out_flat, preferred_element_type=jnp....  56.2 us
    all_gather x1, waiting for transfers between devices, local(): gathered = lax.all_gather(arrived, 'tp', axis=0, tiled=True)  49.7 us
    all_gather x1, waiting for transfers between devices, local(): lax.all_gather(own_values, 'sp', axis=0, tiled=True)  32.6 us
    all_gather x1, waiting for transfers between devices, local(): lax.all_gather(own_keys, 'sp', axis=0, tiled=True)  20.9 us
    dot_general x1, matrix products, local(): jnp.einsum('secf,efd->secd', hidden, down_weight, preferred_element_type=...  16 us
    all_to_all x1, blocking collectives, local(): lax.all_to_all(outgoing, 'sp', split_axis=0, concat_axis=0, tiled=True)  11.4 us
    dot_general x1, matrix products, local(): jnp.einsum('secd,edf->secf', gathered, gate_weight, preferred_element_typ...  10.3 us
  transfers between devices with their start and end apart: 6, of which 6 were waited for; matrix products, arithmetic and copies ran while one was open for 1% of the time, Pallas kernels for 0%

commit v1 on v0

v1 whole, which is shorter than its diff:
```python
import functools

import jax
import jax.numpy as jnp
from jax import lax
from jax.experimental import pallas as pl
from jax.experimental.pallas import tpu as pltpu
from jax.sharding import PartitionSpec as P

DK_A = 64
DV_A = 64
GROUPS = 4

rope_base = 10000.0
epsilon = 1e-06
floor_score = -1e30
MESH = pl.DeviceIdType.MESH
VM = pl.BlockSpec(memory_space=pltpu.VMEM)


def angle_tables(places, rope_width):
    frequencies = rope_base ** (-jnp.arange(0, rope_width, 2, dtype=jnp.float32) / rope_width)
    angles = places[:, None] * frequencies[None, :]
    return (jnp.cos(angles), jnp.sin(angles))


def rms_scale(values, gain_vector):
    values = values.astype(jnp.float32)
    inverse = lax.rsqrt(jnp.mean(values * values, axis=-1, keepdims=True) + epsilon)
    return values * inverse * gain_vector


def greet(targets):
    barrier = pltpu.get_barrier_semaphore()
    for target in targets:
        pl.semaphore_signal(barrier, inc=1, device_id=target, device_id_type=MESH)
    pl.semaphore_wait(barrier, len(targets))


def remote(src, dst, send, recv, target):
    return pltpu.make_async_remote_copy(
        src_ref=src,
        dst_ref=dst,
        send_sem=send,
        recv_sem=recv,
        device_id=target,
        device_id_type=MESH,
    )


def comm_call(kernel, out_shape, scratch, identity, args):
    return pl.pallas_call(
        kernel,
        out_shape=out_shape,
        in_specs=[VM] * len(args),
        out_specs=VM,
        scratch_shapes=scratch,
        compiler_params=pltpu.CompilerParams(
            collective_id=identity, has_side_effects=True, vmem_limit_bytes=48 * 1024 * 1024
        ),
    )(*args)


def gather_sp_kernel(sp_count, x_ref, out_ref, send, recv, fsend, local_sem):
    me = lax.axis_index("sp")
    tp = lax.axis_index("tp")
    core = lax.rem(tp, 2)
    partner = tp + 1 - 2 * core
    half = x_ref.shape[0] // 2
    greet([(lax.rem(me + k, sp_count), tp) for k in range(1, sp_count)] + [(me, partner)])
    mine = pl.ds(pl.multiple_of(core * half, half), half)
    other = pl.ds(pl.multiple_of((1 - core) * half, half), half)
    own = pltpu.make_async_copy(x_ref, out_ref.at[me], local_sem)
    own.start()

    def outgoing(to):
        return remote(
            x_ref.at[mine], out_ref.at[me, mine], send.at[to], recv.at[me, core], (to, tp)
        )

    def incoming(source):
        return remote(
            x_ref.at[mine],
            out_ref.at[source, mine],
            send.at[source],
            recv.at[source, core],
            (source, tp),
        )

    def forward(source):
        return remote(
            out_ref.at[source, mine],
            out_ref.at[source, mine],
            fsend.at[source],
            recv.at[source, core],
            (me, partner),
        )

    def forwarded(source):
        return remote(
            out_ref.at[source, other],
            out_ref.at[source, other],
            fsend.at[source],
            recv.at[source, 1 - core],
            (me, partner),
        )

    for to in reversed(range(sp_count)):

        @pl.when(to > me)
        def _():
            outgoing(to).start()

    for source in reversed(range(sp_count)):

        @pl.when(source < me)
        def _():
            incoming(source).wait_recv()
            forward(source).start()

    own.wait()
    for source in range(sp_count):

        @pl.when(source < me)
        def _():
            forwarded(source).wait_recv()
            forward(source).wait_send()

        @pl.when(source > me)
        def _():
            outgoing(source).wait_send()


def gather_sp(x, sp_count, identity):
    return comm_call(
        functools.partial(gather_sp_kernel, sp_count),
        jax.ShapeDtypeStruct((sp_count,) + x.shape, x.dtype),
        [
            pltpu.SemaphoreType.DMA((sp_count,)),
            pltpu.SemaphoreType.DMA((sp_count, 2)),
            pltpu.SemaphoreType.DMA((sp_count,)),
            pltpu.SemaphoreType.DMA,
        ],
        identity,
        (x,),
    )


def gather_tp_kernel(tp_count, x_ref, out_ref, send, psend, recv, local_sem):
    sp = lax.axis_index("sp")
    tp = lax.axis_index("tp")
    core = lax.rem(tp, 2)
    z = lax.div(tp, 2)
    depth = tp_count // 2
    partner = tp + 1 - 2 * core
    peers = [lax.rem(z + k, depth) * 2 + core for k in range(1, depth)]
    order = sorted(range(depth - 1), key=lambda i: -min(i + 1, depth - 1 - i))
    greet([(sp, partner)] + [(sp, peer) for peer in peers])
    own = pltpu.make_async_copy(x_ref, out_ref.at[tp], local_sem)
    own.start()
    sends = []
    for i in order:
        copy = remote(x_ref, out_ref.at[tp], send.at[i], recv.at[tp], (sp, peers[i]))
        copy.start()
        sends.append(copy)
    copy = remote(x_ref, out_ref.at[tp], psend.at[depth - 1], recv.at[tp], (sp, partner))
    copy.start()
    sends.append(copy)
    for i in reversed(order):
        block = peers[i]
        remote(x_ref, out_ref.at[block], send.at[i], recv.at[block], (sp, block)).wait_recv()
        copy = remote(
            out_ref.at[block], out_ref.at[block], psend.at[i], recv.at[block], (sp, partner)
        )
        copy.start()
        sends.append(copy)
    for k in range(depth):
        block = lax.rem(z + k, depth) * 2 + 1 - core
        remote(x_ref, out_ref.at[block], psend.at[0], recv.at[block], (sp, partner)).wait_recv()
    for copy in sends:
        copy.wait_send()
    own.wait()


def gather_tp(x, tp_count, identity):
    return comm_call(
        functools.partial(gather_tp_kernel, tp_count),
        jax.ShapeDtypeStruct((tp_count,) + x.shape, x.dtype),
        [
            pltpu.SemaphoreType.DMA((tp_count,)),
            pltpu.SemaphoreType.DMA((tp_count,)),
            pltpu.SemaphoreType.DMA((tp_count,)),
            pltpu.SemaphoreType.DMA,
        ],
        identity,
        (x,),
    )


def reduce_tp_kernel(
    tp_count, x_ref, out_ref, partner_in, stage, z_in, send, recv, zsend, zrecv
):
    sp = lax.axis_index("sp")
    tp = lax.axis_index("tp")
    core = lax.rem(tp, 2)
    z = lax.div(tp, 2)
    depth = tp_count // 2
    partner = tp + 1 - 2 * core
    offsets = sorted(range(1, depth), key=lambda k: -min(k, depth - k)) + [0]
    places = [lax.rem(z + k, depth) for k in offsets]
    greet([(sp, partner)] + [(sp, place * 2 + core) for place in places[:-1]])
    swaps = []
    for place in places:
        copy = remote(
            x_ref.at[place * 2 + 1 - core],
            partner_in.at[place],
            send.at[place],
            recv.at[place],
            (sp, partner),
        )
        copy.start()
        swaps.append(copy)
    sends = []
    total = None
    for i, place in enumerate(places):
        swaps[i].wait_recv()
        total = x_ref[place * 2 + core].astype(jnp.float32) + partner_in[place].astype(jnp.float32)
        if i < depth - 1:
            stage[place] = total.astype(stage.dtype)
        else:
            out_ref[...] = total
        if i > 0:
            back = places[i - 1]
            copy = remote(
                stage.at[back], z_in.at[z], zsend.at[back], zrecv.at[z], (sp, back * 2 + core)
            )
            copy.start()
            sends.append(copy)
    for place in reversed(places[:-1]):
        remote(
            stage.at[place], z_in.at[place], zsend.at[place], zrecv.at[place], (sp, place * 2 + core)
        ).wait_recv()
        out_ref[...] += z_in[place].astype(jnp.float32)
    for copy in swaps + sends:
        copy.wait_send()


def reduce_tp(x, tp_count, identity):
    block = x.shape[1:]
    depth = tp_count // 2
    buffer = pltpu.VMEM((depth,) + block, x.dtype)
    return comm_call(
        functools.partial(reduce_tp_kernel, tp_count),
        jax.ShapeDtypeStruct(block, jnp.float32),
        [buffer, buffer, buffer] + [pltpu.SemaphoreType.DMA((depth,))] * 4,
        identity,
        (x,),
    )


def swap_sp_kernel(sp_count, x_ref, out_ref, send, recv, local_sem):
    me = lax.axis_index("sp")
    tp = lax.axis_index("tp")
    others = [lax.rem(me + k, sp_count) for k in range(1, sp_count)]
    greet([(other, tp) for other in others])
    copies = []
    for other in others:
        copy = remote(x_ref.at[other], out_ref.at[me], send.at[other], recv.at[me], (other, tp))
        copy.start()
        copies.append(copy)
    own = pltpu.make_async_copy(x_ref.at[me], out_ref.at[me], local_sem)
    own.start()
    own.wait()
    for other in others:
        remote(
            x_ref.at[other], out_ref.at[other], send.at[other], recv.at[other], (other, tp)
        ).wait_recv()
    for copy in copies:
        copy.wait_send()


def swap_sp(x, sp_count, identity):
    return comm_call(
        functools.partial(swap_sp_kernel, sp_count),
        jax.ShapeDtypeStruct(x.shape, x.dtype),
        [
            pltpu.SemaphoreType.DMA((sp_count,)),
            pltpu.SemaphoreType.DMA((sp_count,)),
            pltpu.SemaphoreType.DMA,
        ],
        identity,
        (x,),
    )


NT = (((1,), (1,)), ((), ()))


def attend_kernel(
    rope_width,
    x_ref,
    q_ref,
    qr_ref,
    cos_ref,
    sin_ref,
    turn_ref,
    wk_ref,
    wv_ref,
    wo_ref,
    out_ref,
    turned,
    keys,
    values,
    tops,
    sums,
    acc,
):
    me = lax.axis_index("sp")
    tokens, width = q_ref.shape
    latent = wk_ref.shape[0]
    pair_width = width // (qr_ref.shape[1] // (2 * rope_width))
    pairs = width // pair_width
    raw = qr_ref[...]
    swapped = jnp.dot(raw, turn_ref[...], preferred_element_type=jnp.float32)
    turned[...] = (raw.astype(jnp.float32) * cos_ref[...] + swapped * sin_ref[...]).astype(
        turned.dtype
    )
    scales = ((DK_A + rope_width) ** (-0.5), (pair_width - DK_A + rope_width) ** (-0.5))

    def block(index, first):
        compressed = x_ref[index, :, :latent]
        rope = x_ref[index, :, latent:]
        keys[...] = jnp.dot(compressed, wk_ref[...], preferred_element_type=jnp.float32).astype(
            keys.dtype
        )
        values[...] = jnp.dot(compressed, wv_ref[...], preferred_element_type=jnp.float32).astype(
            values.dtype
        )
        for pair in range(pairs):
            span = slice(pair * pair_width, (pair + 1) * pair_width)
            lane = lax.broadcasted_iota(jnp.int32, (tokens, pair_width), 1)
            rope_lane = lax.broadcasted_iota(jnp.int32, turned.shape, 1)
            factors, updates = [], []
            for group in range(2):
                head = pair * 2 + group
                chosen = (lane < DK_A) if group == 0 else (lane >= DK_A)
                query = jnp.where(chosen, q_ref[:, span], jnp.zeros((), q_ref.dtype))
                low = head * rope_width
                query_rope = jnp.where(
                    (rope_lane >= low) & (rope_lane < low + rope_width),
                    turned[...],
                    jnp.zeros((), turned.dtype),
                )
                scores = lax.dot_general(
                    query, keys[:, span], NT, preferred_element_type=jnp.float32
                ) + lax.dot_general(query_rope, rope, NT, preferred_element_type=jnp.float32)
                scores = scores * scales[group]
                if first:
                    row = lax.broadcasted_iota(jnp.int32, (tokens, tokens), 0)
                    column = lax.broadcasted_iota(jnp.int32, (tokens, tokens), 1)
                    scores = jnp.where(row >= column, scores, floor_score)
                    top = jnp.max(scores, axis=1, keepdims=True)
                else:
                    old = tops[head]
                    top = jnp.maximum(old, jnp.max(scores, axis=1, keepdims=True))
                    factors.append(jnp.exp(old - top))
                weights = jnp.exp(scores - top)
                total = jnp.sum(weights, axis=1, keepdims=True)
                tops[head] = top
                sums[head] = total if first else sums[head] * factors[-1] + total
                updates.append(
                    jnp.dot(
                        weights.astype(values.dtype),
                        values[:, span],
                        preferred_element_type=jnp.float32,
                    )
                )
            value_lane = lane < DV_A
            update = jnp.where(value_lane, updates[0], updates[1])
            if first:
                acc[:, span] = update
            else:
                acc[:, span] = (
                    acc[:, span] * jnp.where(value_lane, factors[0], factors[1]) + update
                )

    block(me, True)

    def step(index, unused):
        block(index, False)
        return unused

    lax.fori_loop(0, me, step, 0)
    for pair in range(pairs):
        span = slice(pair * pair_width, (pair + 1) * pair_width)
        lane = lax.broadcasted_iota(jnp.int32, (tokens, pair_width), 1)
        bottom = jnp.where(lane < DV_A, sums[pair * 2], sums[pair * 2 + 1])
        keys[:, span] = (acc[:, span] / bottom).astype(keys.dtype)
    piece = 512
    for start in range(0, wo_ref.shape[1], piece):
        out_ref[:, start : start + piece] = jnp.dot(
            keys[...], wo_ref[:, start : start + piece], preferred_element_type=jnp.float32
        ).astype(out_ref.dtype)


def local(
    residual,
    queries,
    query_rope,
    latent,
    key_rope,
    latent_gain,
    key_weight,
    value_weight,
    out_weight,
    norm_gain,
    routes,
    group_gate,
    expert_share,
    gate_weight,
    up_weight,
    down_weight,
):
    tokens = queries.shape[0]
    pair_dev = queries.shape[1]
    sp_count = lax.axis_size("sp")
    tp_count = lax.axis_size("tp")
    row_count = tokens // tp_count
    rope_width = key_rope.shape[1]
    half = rope_width // 2
    copies = pair_dev * 2
    latent_width = latent.shape[1]
    model = residual.shape[1]
    low = jnp.bfloat16

    first_place = lax.axis_index("sp") * tokens
    places = (first_place + jnp.arange(tokens, dtype=jnp.int32)).astype(jnp.float32)
    cosine, sine = angle_tables(places, rope_width)
    cosine = jnp.tile(cosine, (1, 2 * copies))
    sine = jnp.tile(sine, (1, 2 * copies))
    index = jnp.arange(copies * rope_width, dtype=jnp.int32)
    source = jnp.where(index % rope_width < half, index + half, index - half)
    sign = jnp.where(index % rope_width < half, -1.0, 1.0)
    turn = jnp.where(index[:, None] == source[None, :], sign[None, :], 0.0).astype(low)
    key_raw = jnp.tile(key_rope, (1, copies))
    rotated = (
        key_raw.astype(jnp.float32) * cosine
        + jnp.dot(key_raw, turn, preferred_element_type=jnp.float32) * sine
    ).astype(low)
    compressed = rms_scale(latent, latent_gain).astype(low)
    gathered = gather_sp(jnp.concatenate([compressed, rotated], axis=1), sp_count, 0)

    width = pair_dev * queries.shape[2]
    scratch = [
        pltpu.VMEM((tokens, copies * rope_width), low),
        pltpu.VMEM((tokens, width), low),
        pltpu.VMEM((tokens, width), low),
        pltpu.VMEM((copies, tokens, 1), jnp.float32),
        pltpu.VMEM((copies, tokens, 1), jnp.float32),
        pltpu.VMEM((tokens, width), jnp.float32),
    ]
    partial = pl.pallas_call(
        functools.partial(attend_kernel, rope_width),
        out_shape=jax.ShapeDtypeStruct((tokens, model), low),
        in_specs=[VM] * 9,
        out_specs=VM,
        scratch_shapes=scratch,
        compiler_params=pltpu.CompilerParams(vmem_limit_bytes=56 * 1024 * 1024),
    )(
        gathered,
        queries.reshape(tokens, width),
        query_rope.reshape(tokens, copies * rope_width),
        cosine,
        sine,
        turn,
        key_weight.reshape(latent_width, -1),
        value_weight.reshape(latent_width, -1),
        out_weight.reshape(width, model),
    )
    head_total = reduce_tp(partial.reshape(tp_count, row_count, model), tp_count, 1)
    mixed_rows = residual.astype(jnp.float32) + head_total
    normed = rms_scale(mixed_rows, norm_gain).astype(low)

    experts_dev = gate_weight.shape[0]
    experts_all = experts_dev * sp_count
    top_count = routes.shape[1]
    capacity = max(2, 3 * row_count * top_count // (2 * experts_all))
    slots = experts_dev * capacity
    if experts_all // GROUPS == experts_dev == top_count:
        slots = capacity
    own = lax.dynamic_slice_in_dim(routes, lax.axis_index("tp") * row_count, row_count, 0)
    route_weight = group_gate[:, None] * expert_share / jnp.sum(expert_share, axis=1, keepdims=True)
    expert_ids = jnp.arange(experts_all, dtype=jnp.int32)
    named = own[:, :, None] == expert_ids[None, None, :]
    table = jnp.sum(jnp.where(named, route_weight[:, :, None], 0.0), axis=1)
    member = jnp.any(named, axis=1).reshape(row_count, sp_count, experts_dev).any(axis=2)
    counted = member.astype(jnp.int32)
    rank = jnp.cumsum(counted, axis=0) - counted
    slot_ids = jnp.arange(slots, dtype=jnp.int32)
    pick = (rank.T[:, None, :] == slot_ids[None, :, None]) & member.T[:, None, :]
    slot_weight = jnp.sum(
        jnp.where(
            pick[:, :, None, :],
            table.reshape(row_count, sp_count, experts_dev).transpose(1, 2, 0)[:, None],
            0.0,
        ),
        axis=3,
    )
    weight_high = slot_weight.astype(low)
    weight_low = (slot_weight - weight_high.astype(jnp.float32)).astype(low)
    pick_matrix = pick.astype(low).reshape(sp_count * slots, row_count)
    outgoing = jnp.dot(pick_matrix, normed, preferred_element_type=jnp.float32).astype(low)
    extra = jnp.concatenate([weight_high, weight_low], axis=2)
    extra = jnp.pad(extra, ((0, 0), (0, 0), (0, 128 - extra.shape[2])))
    outgoing = jnp.concatenate([outgoing.reshape(sp_count, slots, model), extra], axis=2)
    arrived = swap_sp(outgoing, sp_count, 2)
    rows = sp_count * slots
    everyone = gather_tp(arrived.reshape(rows, model + 128), tp_count, 3)
    everyone = everyone.reshape(tp_count * rows, model + 128)
    inputs = everyone[:, :model]
    tail = everyone[:, model : model + 2 * experts_dev].astype(jnp.float32)
    scale = tail[:, :experts_dev] + tail[:, experts_dev:]
    gate_out = jnp.einsum("rd,edf->erf", inputs, gate_weight, preferred_element_type=jnp.float32)
    up_out = jnp.einsum("rd,edf->erf", inputs, up_weight, preferred_element_type=jnp.float32)
    hidden = (jax.nn.silu(gate_out) * up_out * scale.T[:, :, None]).astype(low)
    expert_part = jnp.einsum(
        "erf,efd->rd", hidden, down_weight, preferred_element_type=jnp.float32
    ).astype(low)
    expert_out = reduce_tp(expert_part.reshape(tp_count, rows, model), tp_count, 4).astype(low)
    returned = swap_sp(expert_out.reshape(sp_count, slots, model), sp_count, 5)
    expert_mix = jnp.dot(
        pick_matrix.T, returned.reshape(rows, model), preferred_element_type=jnp.float32
    )
    return (mixed_rows + expert_mix).astype(low)


def solution(mesh):
    return jax.shard_map(
        local,
        mesh=mesh,
        in_specs=(
            P(("sp", "tp"), None),
            P("sp", "tp", None),
            P("sp", "tp", None),
            P("sp", None),
            P("sp", None),
            P(),
            P(None, "tp", None),
            P(None, "tp", None),
            P("tp", None, None),
            P(),
            P("sp", None),
            P(("sp", "tp")),
            P(("sp", "tp"), None),
            P("sp", None, "tp"),
            P("sp", None, "tp"),
            P("sp", "tp", None),
        ),
        out_specs=P(("sp", "tp"), None),
        check_vma=False,
    )
```

time: 375 us -> 170 us (0.45)
  the two profiles are of different devices: /device:TPU:0 before, /device:TPU:16 now
where the time goes in v1:
time: 170 us
  Pallas kernels  135 us (79%)
  matrix products  18.5 us (11%)
  local copies, waits for them, and re-layouts  11.8 us (7%)
  other arithmetic  4.34 us (3%)
    pallas_call x6, Pallas kernels, comm_call(): pl.pallas_call(kernel, out_shape=out_shape, in_specs=[VM] * len(args), ou...  127 us
    dot_general x1, matrix products, local(): jnp.einsum('erf,efd->rd', hidden, down_weight, preferred_element_type=jnp...  10.8 us
    unnamed x29, local copies, waits for them, and re-layouts  7.61 us
    pallas_call x1, Pallas kernels, local(): pl.pallas_call(functools.partial(attend_kernel, rope_width), out_shape=ja...  7.52 us
    dot_general x1, matrix products, local(): jnp.einsum('rd,edf->erf', inputs, up_weight, preferred_element_type=jnp.f...  6.25 us

profile of v1, /device:TPU:16, one launch (start us, length us, event | category | flops | bytes accessed | tf_op | source)
XLA Modules:
  0.0 169.6 jit_solution(9087015335401876914)
XLA Ops:
  0.0 0.7 copy-done
  0.8 0.7 reduce_sum.47
  1.5 0.7 multiply_divide_fusion
  2.3 1.2 fusion.12
  3.9 0.1 select_reduce_fusion
  4.1 0.1 copy.99
  4.2 0.3 copy.97
  4.5 0.6 select_convert_fusion.turn_ref
  5.1 0.2 multiply_cosine_fusion
  5.5 1.6 copy.89.qr_ref
  7.2 0.7 tile.12
  8.4 0.2 fusion.11
  8.7 0.2 fusion.14
  8.9 0.8 copy.102
  9.7 0.9 copy.103
  10.6 0.9 copy.104
  11.4 13.4 %shard_map.154.x_ref = bf16[4,384,640]{2,1,0:T(8,128)(2,1)S(1)} custom-call(bf16[384,640]{1,0:T(8,128)(2,1)S(1)} %pad_maximum_fusion.x_ref), custom_call_target="tpu_custom_call" | custom-call | tf_op jit(solution)/shard_map/pallas_call | solution.py:52
  24.9 1.3 copy-done.1
  26.2 7.5 %shard_map.155 = bf16[384,2048]{1,0:T(8,128)(2,1)} custom-call(bf16[4,384,640]{2,1,0:T(8,128)(2,1)} %copy-done.1, bf16[384,512]{1,0:T(8,128)(2,1)} %bitcast.85, bf16[384,128]{1,0:T(8,128)(2,1)} %copy.89.qr_ref, f32[384,128]{1,0:T(8,128)} %copy-done.5, f32[384,128]{1,0:T(8,128)} %copy-done.6, bf16[128,128]{1,0:T(8,128)(2,1)} %select_convert_fusion.turn_ref, ...), custom_call_target="tpu_custom_call" | custom-call | tf_op jit(solution)/shard_map/pallas_call | solution.py:462
  33.7 1.4 copy-done.2
  35.1 22.5 %shard_map.156 = f32[48,2048]{1,0:T(8,128)S(1)} custom-call(bf16[8,48,2048]{2,1,0:T(8,128)(2,1)S(1)} %bitcast.77), custom_call_target="tpu_custom_call" | custom-call | tf_op jit(solution)/shard_map/pallas_call | solution.py:52
  57.7 0.2 multiply_reduce_fusion
  57.9 0.3 convolution_convert_fusion
  58.3 20.9 %shard_map.157 = bf16[4,18,2176]{2,1,0:T(8,128)(2,1)S(1)} custom-call(bf16[4,18,2176]{2,1,0:T(8,128)(2,1)S(1)} %pad_maximum_fusion.1.x_ref), custom_call_target="tpu_custom_call" | custom-call | tf_op jit(solution)/shard_map/pallas_call | solution.py:52
  79.3 31.7 %shard_map.158 = bf16[8,72,2176]{2,1,0:T(8,128)(2,1)S(1)} custom-call(bf16[72,2176]{1,0:T(8,128)(2,1)S(1)} %reshape.178.x_ref), custom_call_target="tpu_custom_call" | custom-call | tf_op jit(solution)/shard_map/pallas_call | solution.py:52
  111.0 0.1 fusion.15
  111.3 6.2 %fusion.7 = f32[576,2,512]{2,0,1:T(8,128)} fusion(bf16[2,2048,512]{2,1,0:T(8,128)(2,1)} %param.30, bf16[576,2176]{1,0:T(8,128)(2,1)S(1)} %bitcast.79), kind=kOutput, calls=%fused_computation.14 | convolution fusion | flops 2415919104 | bytes 8912896 | tf_op jit(solution)/shard_map/rd,edf->erf/dot_general | solution.py:524
  117.5 10.8 %bitcast_convert_fusion = bf16[576,2048]{1,0:T(8,128)(2,1)} fusion(bf16[2,512,2048]{2,1,0:T(8,128)(2,1)} %param.31, f32[576,2,512]{2,0,1:T(8,128)} %fusion.7, bf16[2,2048,512]{2,1,0:T(8,128)(2,1)} %param.29, bf16[576,2176]{1,0:T(8,128)(2,1)S(1)} %bitcast.80, f32[2,576]{1,0:T(2,128)S(1)} %copy.100), kind=kOutput, calls=%fused_computation | convolution fusion | flops 4837146624 | bytes 15471616 | tf_op jit(solution)/shard_map/erf,efd->rd/dot_general | solution.py:526
  128.4 1.7 copy-done.3
  130.0 30.5 %shard_map.159 = f32[72,2048]{1,0:T(8,128)S(1)} custom-call(bf16[8,72,2048]{2,1,0:T(8,128)(2,1)S(1)} %bitcast.81), custom_call_target="tpu_custom_call" | custom-call | tf_op jit(solution)/shard_map/pallas_call | solution.py:52
  160.7 8.0 %shard_map.160 = bf16[4,18,2048]{2,1,0:T(8,128)(2,1)S(1)} custom-call(bf16[4,18,2048]{2,1,0:T(8,128)(2,1)S(1)} %reshape.181.x_ref), custom_call_target="tpu_custom_call" | custom-call | tf_op jit(solution)/shard_map/pallas_call | solution.py:52
  168.7 0.9 fusion.6
  (64 shorter events, 1.9 us)
Async XLA Ops:
  0.0 0.7 copy-start
  0.0 8.6 %copy-start.7 = (bf16[384,512]{1,0:T(8,128)(2,1)S(1)}, bf16[384,512]{1,0:T(8,128)(2,1)}, u32[]{:S(2)}) copy-start(bf16[384,512]{1,0:T(8,128)(2,1)} %param.19) | copy-start | bytes 1179652
  0.0 8.6 %copy-start.12 = (f32[512]{0:T(512)S(1)}, f32[512]{0:T(512)}, u32[]{:S(2)}) copy-start(f32[512]{0:T(512)} %param.21) | copy-start | bytes 6148
  4.5 4.4 %copy-start.10 = (bf16[384,2,256]{2,1,0:T(2,128)(2,1)S(1)}, bf16[384,2,256]{2,1,0:T(2,128)(2,1)}, u32[]{:S(2)}) copy-start(bf16[384,2,256]{2,1,0:T(2,128)(2,1)} %param.17) | copy-start | bytes 1179652
  7.9 1.8 %copy-start.8 = (bf16[512,2,256]{2,1,0:T(2,128)(2,1)S(1)}, bf16[512,2,256]{2,1,0:T(2,128)(2,1)}, u32[]{:S(2)}) copy-start(bf16[512,2,256]{2,1,0:T(2,128)(2,1)} %param.22) | copy-start | bytes 1572868
  8.2 2.4 %copy-start.5 = (f32[384,128]{1,0:T(8,128)}, f32[384,128]{1,0:T(8,128)S(1)}, u32[]{:S(2)}) copy-start(f32[384,128]{1,0:T(8,128)S(1)} %copy.86.cos_ref) | copy-start | bytes 589828
  8.2 2.3 %copy-start.9 = (bf16[512,2,256]{2,1,0:T(2,128)(2,1)S(1)}, bf16[512,2,256]{2,1,0:T(2,128)(2,1)}, u32[]{:S(2)}) copy-start(bf16[512,2,256]{2,1,0:T(2,128)(2,1)} %param.23) | copy-start | bytes 1572868
  8.4 3.1 %copy-start.6 = (f32[384,128]{1,0:T(8,128)}, f32[384,128]{1,0:T(8,128)S(1)}, u32[]{:S(2)}) copy-start(f32[384,128]{1,0:T(8,128)S(1)} %copy.88.sin_ref) | copy-start | bytes 589828
  24.9 1.3 copy-start.1
  26.2 31.5 %copy-start.4 = (bf16[48,2048]{1,0:T(8,128)(2,1)S(1)}, bf16[48,2048]{1,0:T(8,128)(2,1)}, u32[]{:S(2)}) copy-start(bf16[48,2048]{1,0:T(8,128)(2,1)} %param.16) | copy-start | bytes 589828
  33.7 1.4 copy-start.2
  35.1 22.7 %copy-start.11 = (f32[2048]{0:T(1024)S(1)}, f32[2048]{0:T(1024)}, u32[]{:S(2)}) copy-start(f32[2048]{0:T(1024)} %param.25) | copy-start | bytes 24580
  128.4 1.7 copy-start.3

commit v2 on v1

--- a/solution.py
+++ b/solution.py
@@ -61,188 +61,267 @@
     )(*args)
 
 
-def gather_sp_kernel(sp_count, x_ref, out_ref, send, recv, fsend, local_sem):
-    me = lax.axis_index("sp")
-    tp = lax.axis_index("tp")
-    core = lax.rem(tp, 2)
-    partner = tp + 1 - 2 * core
-    half = x_ref.shape[0] // 2
-    greet([(lax.rem(me + k, sp_count), tp) for k in range(1, sp_count)] + [(me, partner)])
-    mine = pl.ds(pl.multiple_of(core * half, half), half)
-    other = pl.ds(pl.multiple_of((1 - core) * half, half), half)
-    own = pltpu.make_async_copy(x_ref, out_ref.at[me], local_sem)
-    own.start()
-
-    def outgoing(to):
-        return remote(
-            x_ref.at[mine], out_ref.at[me, mine], send.at[to], recv.at[me, core], (to, tp)
-        )
-
-    def incoming(source):
-        return remote(
-            x_ref.at[mine],
-            out_ref.at[source, mine],
-            send.at[source],
-            recv.at[source, core],
-            (source, tp),
-        )
-
-    def forward(source):
-        return remote(
-            out_ref.at[source, mine],
-            out_ref.at[source, mine],
-            fsend.at[source],
-            recv.at[source, core],
-            (me, partner),
-        )
-
-    def forwarded(source):
-        return remote(
-            out_ref.at[source, other],
-            out_ref.at[source, other],
-            fsend.at[source],
-            recv.at[source, 1 - core],
-            (me, partner),
-        )
-
-    for to in reversed(range(sp_count)):
-
-        @pl.when(to > me)
-        def _():
-            outgoing(to).start()
-
-    for source in reversed(range(sp_count)):
-
-        @pl.when(source < me)
-        def _():
-            incoming(source).wait_recv()
-            forward(source).start()
-
-    own.wait()
-    for source in range(sp_count):
-
-        @pl.when(source < me)
-        def _():
-            forwarded(source).wait_recv()
-            forward(source).wait_send()
-
-        @pl.when(source > me)
-        def _():
-            outgoing(source).wait_send()
-
-
-def gather_sp(x, sp_count, identity):
-    return comm_call(
-        functools.partial(gather_sp_kernel, sp_count),
-        jax.ShapeDtypeStruct((sp_count,) + x.shape, x.dtype),
-        [
-            pltpu.SemaphoreType.DMA((sp_count,)),
-            pltpu.SemaphoreType.DMA((sp_count, 2)),
-            pltpu.SemaphoreType.DMA((sp_count,)),
-            pltpu.SemaphoreType.DMA,
-        ],
-        identity,
-        (x,),
-    )
-
-
-def gather_tp_kernel(tp_count, x_ref, out_ref, send, psend, recv, local_sem):
+def greet_some(targets):
+    barrier = pltpu.get_barrier_semaphore()
+    count = 0
+    for here, target in targets:
+
+        @pl.when(here)
+        def _():
+            pl.semaphore_signal(barrier, inc=1, device_id=target, device_id_type=MESH)
+
+        count = count + jnp.where(here, 1, 0)
+    pl.semaphore_wait(barrier, count)
+
+
+def line(tp_count):
     sp = lax.axis_index("sp")
     tp = lax.axis_index("tp")
     core = lax.rem(tp, 2)
     z = lax.div(tp, 2)
     depth = tp_count // 2
-    partner = tp + 1 - 2 * core
-    peers = [lax.rem(z + k, depth) * 2 + core for k in range(1, depth)]
-    order = sorted(range(depth - 1), key=lambda i: -min(i + 1, depth - 1 - i))
-    greet([(sp, partner)] + [(sp, peer) for peer in peers])
-    own = pltpu.make_async_copy(x_ref, out_ref.at[tp], local_sem)
-    own.start()
-    sends = []
-    for i in order:
-        copy = remote(x_ref, out_ref.at[tp], send.at[i], recv.at[tp], (sp, peers[i]))
-        copy.start()
-        sends.append(copy)
-    copy = remote(x_ref, out_ref.at[tp], psend.at[depth - 1], recv.at[tp], (sp, partner))
-    copy.start()
-    sends.append(copy)
-    for i in reversed(order):
-        block = peers[i]
-        remote(x_ref, out_ref.at[block], send.at[i], recv.at[block], (sp, block)).wait_recv()
-        copy = remote(
-            out_ref.at[block], out_ref.at[block], psend.at[i], recv.at[block], (sp, partner)
-        )
-        copy.start()
-        sends.append(copy)
-    for k in range(depth):
-        block = lax.rem(z + k, depth) * 2 + 1 - core
-        remote(x_ref, out_ref.at[block], psend.at[0], recv.at[block], (sp, partner)).wait_recv()
-    for copy in sends:
-        copy.wait_send()
-    own.wait()
-
-
-def gather_tp(x, tp_count, identity):
-    return comm_call(
-        functools.partial(gather_tp_kernel, tp_count),
-        jax.ShapeDtypeStruct((tp_count,) + x.shape, x.dtype),
-        [
-            pltpu.SemaphoreType.DMA((tp_count,)),
-            pltpu.SemaphoreType.DMA((tp_count,)),
-            pltpu.SemaphoreType.DMA((tp_count,)),
-            pltpu.SemaphoreType.DMA,
+    partner = (sp, tp + 1 - 2 * core)
+    return sp, core, z, depth, partner, (sp, tp + 2), (sp, tp - 2), z < depth - 1, z > 0
+
+
+def expert_kernel(
+    tp_count,
+    x_ref,
+    gate_ref,
+    up_ref,
+    down_ref,
+    out_ref,
+    held,
+    gate,
+    up,
+    down,
+    usend,
+    dsend,
+    psend,
+    recv,
+    wsem,
+):
+    sp, core, z, depth, partner, above, below, has_above, has_below = line(tp_count)
+    tp = lax.axis_index("tp")
+    experts = gate_ref.shape[0]
+    model = gate_ref.shape[1]
+    rows = x_ref.shape[0]
+    loads = [
+        pltpu.make_async_copy(source, target, wsem.at[i])
+        for i, (source, target) in enumerate(((gate_ref, gate), (up_ref, up), (down_ref, down)))
+    ]
+    for load in loads:
+        load.start()
+    greet_some([(True, partner), (has_above, above), (has_below, below)])
+
+    def move(block, sem, target, source=None):
+        source = held.at[block] if source is None else source
+        return remote(source, held.at[block], sem, recv.at[block], target)
+
+    @pl.when(has_above)
+    def _():
+        move(tp, usend.at[z], above, x_ref).start()
+
+    @pl.when(has_below)
+    def _():
+        move(tp, dsend.at[z], below, x_ref).start()
+
+    move(tp, psend.at[z], partner, x_ref).start()
+    held[tp] = x_ref[...]
+
+    def take(k):
+        low, high = z - k, z + k
+
+        @pl.when(low >= 0)
+        def _():
+            block = low * 2 + core
+            move(block, usend.at[low], partner).wait_recv()
+
+            @pl.when(has_above)
+            def _():
+                move(block, usend.at[low], above).start()
+
+            move(block, psend.at[low], partner).start()
+
+        @pl.when(high < depth)
+        def _():
+            block = high * 2 + core
+            move(block, dsend.at[high], partner).wait_recv()
+
+            @pl.when(has_below)
+            def _():
+                move(block, dsend.at[high], below).start()
+
+            move(block, psend.at[high], partner).start()
+
+    def compute(place):
+        move(place * 2 + 1 - core, psend.at[place], partner).wait_recv()
+        blocks = pl.ds(place * 2, 2)
+        x = held[blocks].reshape(2 * rows, held.shape[2])
+        inputs = x[:, :model]
+        tail = x[:, model:].astype(jnp.float32)
+        total = None
+        for e in range(experts):
+            scale = tail[:, e : e + 1] + tail[:, experts + e : experts + e + 1]
+            gate_out = jnp.dot(inputs, gate[e], preferred_element_type=jnp.float32)
+            up_out = jnp.dot(inputs, up[e], preferred_element_type=jnp.float32)
+            hidden = (jax.nn.silu(gate_out) * up_out * scale).astype(inputs.dtype)
+            part = jnp.dot(hidden, down[e], preferred_element_type=jnp.float32)
+            total = part if e == 0 else total + part
+        out_ref[blocks] = total.astype(out_ref.dtype).reshape(2, rows, model)
+
+    if depth > 1:
+        take(1)
+    for load in loads:
+        load.wait()
+
+    side = jnp.where(z * 2 >= depth, -1, 1)
+
+    def step(k, unused):
+        one, two = z + side * k, z - side * k
+
+        @pl.when((one >= 0) & (one < depth))
+        def _():
+            compute(one)
+
+        @pl.when((k > 0) & (k + 1 < depth))
+        def _():
+            take(k + 1)
+
+        @pl.when((k > 0) & (two >= 0) & (two < depth))
+        def _():
+            compute(two)
+
+        return unused
+
+    lax.fori_loop(0, depth, step, 0)
+    for place in range(depth):
+
+        @pl.when(has_above & (place <= z))
+        def _():
+            move(place * 2 + core, usend.at[place], above).wait_send()
+
+        @pl.when(has_below & (place >= z))
+        def _():
+            move(place * 2 + core, dsend.at[place], below).wait_send()
+
+        move(place * 2 + core, psend.at[place], partner).wait_send()
+
+
+def experts_over_tp(x, gate_weight, up_weight, down_weight, tp_count, identity):
+    dma = pltpu.SemaphoreType.DMA
+    depth = tp_count // 2
+    model = gate_weight.shape[1]
+    anywhere = pl.BlockSpec(memory_space=pl.ANY)
+    return pl.pallas_call(
+        functools.partial(expert_kernel, tp_count),
+        out_shape=jax.ShapeDtypeStruct((tp_count, x.shape[0], model), x.dtype),
+        in_specs=[VM, anywhere, anywhere, anywhere],
+        out_specs=VM,
+        scratch_shapes=[
+            pltpu.VMEM((tp_count,) + x.shape, x.dtype),
+            pltpu.VMEM(gate_weight.shape, gate_weight.dtype),
+            pltpu.VMEM(up_weight.shape, up_weight.dtype),
+            pltpu.VMEM(down_weight.shape, down_weight.dtype),
+            dma((depth,)),
+            dma((depth,)),
+            dma((depth,)),
+            dma((tp_count,)),
+            dma((3,)),
         ],
-        identity,
-        (x,),
-    )
+        compiler_params=pltpu.CompilerParams(
+            collective_id=identity, has_side_effects=True, vmem_limit_bytes=48 * 1024 * 1024
+        ),
+    )(x, gate_weight, up_weight, down_weight)
 
 
 def reduce_tp_kernel(
-    tp_count, x_ref, out_ref, partner_in, stage, z_in, send, recv, zsend, zrecv
+    tp_count, x_ref, out_ref, partner_in, stage, up_in, down_in, send, recv, zsend, urecv, drecv
 ):
-    sp = lax.axis_index("sp")
-    tp = lax.axis_index("tp")
-    core = lax.rem(tp, 2)
-    z = lax.div(tp, 2)
-    depth = tp_count // 2
-    partner = tp + 1 - 2 * core
-    offsets = sorted(range(1, depth), key=lambda k: -min(k, depth - k)) + [0]
-    places = [lax.rem(z + k, depth) for k in offsets]
-    greet([(sp, partner)] + [(sp, place * 2 + core) for place in places[:-1]])
-    swaps = []
-    for place in places:
-        copy = remote(
+    sp, core, z, depth, partner, above, below, has_above, has_below = line(tp_count)
+    greet_some([(True, partner), (has_above, above), (has_below, below)])
+
+    def swap(place):
+        return remote(
             x_ref.at[place * 2 + 1 - core],
             partner_in.at[place],
             send.at[place],
             recv.at[place],
-            (sp, partner),
-        )
-        copy.start()
-        swaps.append(copy)
-    sends = []
-    total = None
-    for i, place in enumerate(places):
-        swaps[i].wait_recv()
-        total = x_ref[place * 2 + core].astype(jnp.float32) + partner_in[place].astype(jnp.float32)
-        if i < depth - 1:
-            stage[place] = total.astype(stage.dtype)
-        else:
-            out_ref[...] = total
-        if i > 0:
-            back = places[i - 1]
-            copy = remote(
-                stage.at[back], z_in.at[z], zsend.at[back], zrecv.at[z], (sp, back * 2 + core)
-            )
-            copy.start()
-            sends.append(copy)
-    for place in reversed(places[:-1]):
-        remote(
-            stage.at[place], z_in.at[place], zsend.at[place], zrecv.at[place], (sp, place * 2 + core)
-        ).wait_recv()
-        out_ref[...] += z_in[place].astype(jnp.float32)
-    for copy in swaps + sends:
-        copy.wait_send()
+            partner,
+        )
+
+    def up(place):
+        return remote(
+            stage.at[place], up_in.at[place], zsend.at[place], urecv.at[place], above
+        )
+
+    def down(place):
+        return remote(
+            stage.at[place], down_in.at[place], zsend.at[place], drecv.at[place], below
+        )
+
+    def pair_sum(place):
+        swap(place).wait_recv()
+        return x_ref[place * 2 + core].astype(jnp.float32) + partner_in[place].astype(jnp.float32)
+
+    for j in range(depth):
+        swap(depth - 1 - j).start()
+        if depth - 1 - j > j:
+            swap(j).start()
+        if depth - 1 - j <= j + 1:
+            break
+
+    for j in range(depth - 1):
+        high, low = depth - 1 + z - j, j + z + 1 - depth
+
+        @pl.when(z <= j)
+        def _():
+            stage[high] = pair_sum(high).astype(stage.dtype)
+
+            @pl.when(has_below)
+            def _():
+                up(high).wait_recv()
+                stage[high] = (
+                    stage[high].astype(jnp.float32) + up_in[high].astype(jnp.float32)
+                ).astype(stage.dtype)
+
+            up(high).start()
+
+        @pl.when(low >= 0)
+        def _():
+            stage[low] = pair_sum(low).astype(stage.dtype)
+
+            @pl.when(has_above)
+            def _():
+                down(low).wait_recv()
+                stage[low] = (
+                    stage[low].astype(jnp.float32) + down_in[low].astype(jnp.float32)
+                ).astype(stage.dtype)
+
+            down(low).start()
+
+    out_ref[...] = pair_sum(z)
+
+    @pl.when(has_below)
+    def _():
+        up(z).wait_recv()
+        out_ref[...] += up_in[z].astype(jnp.float32)
+
+    @pl.when(has_above)
+    def _():
+        down(z).wait_recv()
+        out_ref[...] += down_in[z].astype(jnp.float32)
+
+    for place in range(depth):
+        swap(place).wait_send()
+
+        @pl.when(place > z)
+        def _():
+            up(place).wait_send()
+
+        @pl.when(place < z)
+        def _():
+            down(place).wait_send()
 
 
 def reduce_tp(x, tp_count, identity):
@@ -252,7 +331,7 @@
     return comm_call(
         functools.partial(reduce_tp_kernel, tp_count),
         jax.ShapeDtypeStruct(block, jnp.float32),
-        [buffer, buffer, buffer] + [pltpu.SemaphoreType.DMA((depth,))] * 4,
+        [buffer] * 4 + [pltpu.SemaphoreType.DMA((depth,))] * 5,
         identity,
         (x,),
     )
@@ -298,6 +377,7 @@
 
 def attend_kernel(
     rope_width,
+    sp_count,
     x_ref,
     q_ref,
     qr_ref,
@@ -314,9 +394,55 @@
     tops,
     sums,
     acc,
+    held,
+    send,
+    recv,
+    fsend,
 ):
     me = lax.axis_index("sp")
+    tp = lax.axis_index("tp")
+    core = lax.rem(tp, 2)
+    partner = (me, tp + 1 - 2 * core)
     tokens, width = q_ref.shape
+    half = tokens // 2
+    greet([(lax.rem(me + k, sp_count), tp) for k in range(1, sp_count)] + [partner])
+    mine = pl.ds(pl.multiple_of(core * half, half), half)
+    other = pl.ds(pl.multiple_of((1 - core) * half, half), half)
+
+    def outgoing(to):
+        return remote(
+            x_ref.at[mine], held.at[me, mine], send.at[to], recv.at[me, core], (to, tp)
+        )
+
+    def incoming(source):
+        return remote(
+            x_ref.at[mine], held.at[source, mine], send.at[source], recv.at[source, core], partner
+        )
+
+    def forward(source):
+        return remote(
+            held.at[source, mine],
+            held.at[source, mine],
+            fsend.at[source],
+            recv.at[source, core],
+            partner,
+        )
+
+    def forwarded(source):
+        return remote(
+            held.at[source, other],
+            held.at[source, other],
+            fsend.at[source],
+            recv.at[source, 1 - core],
+            partner,
+        )
+
+    for to in reversed(range(sp_count)):
+
+        @pl.when(to > me)
+        def _():
+            outgoing(to).start()
+
     latent = wk_ref.shape[0]
     pair_width = width // (qr_ref.shape[1] // (2 * rope_width))
     pairs = width // pair_width
@@ -328,8 +454,8 @@
     scales = ((DK_A + rope_width) ** (-0.5), (pair_width - DK_A + rope_width) ** (-0.5))
 
     def block(index, first):
-        compressed = x_ref[index, :, :latent]
-        rope = x_ref[index, :, latent:]
+        compressed = x_ref[:, :latent] if first else held[index, :, :latent]
+        rope = x_ref[:, latent:] if first else held[index, :, latent:]
         keys[...] = jnp.dot(compressed, wk_ref[...], preferred_element_type=jnp.float32).astype(
             keys.dtype
         )
@@ -386,7 +512,11 @@
 
     block(me, True)
 
-    def step(index, unused):
+    def step(i, unused):
+        index = me - 1 - i
+        incoming(index).wait_recv()
+        forward(index).start()
+        forwarded(index).wait_recv()
         block(index, False)
         return unused
 
@@ -401,6 +531,15 @@
         out_ref[:, start : start + piece] = jnp.dot(
             keys[...], wo_ref[:, start : start + piece], preferred_element_type=jnp.float32
         ).astype(out_ref.dtype)
+    for place in range(sp_count):
+
+        @pl.when(place < me)
+        def _():
+            forward(place).wait_send()
+
+        @pl.when(place > me)
+        def _():
+            outgoing(place).wait_send()
 
 
 def local(
@@ -448,7 +587,7 @@
         + jnp.dot(key_raw, turn, preferred_element_type=jnp.float32) * sine
     ).astype(low)
     compressed = rms_scale(latent, latent_gain).astype(low)
-    gathered = gather_sp(jnp.concatenate([compressed, rotated], axis=1), sp_count, 0)
+    own_latent = jnp.concatenate([compressed, rotated], axis=1)
 
     width = pair_dev * queries.shape[2]
     scratch = [
@@ -458,16 +597,22 @@
         pltpu.VMEM((copies, tokens, 1), jnp.float32),
         pltpu.VMEM((copies, tokens, 1), jnp.float32),
         pltpu.VMEM((tokens, width), jnp.float32),
+        pltpu.VMEM((sp_count,) + own_latent.shape, low),
+        pltpu.SemaphoreType.DMA((sp_count,)),
+        pltpu.SemaphoreType.DMA((sp_count, 2)),
+        pltpu.SemaphoreType.DMA((sp_count,)),
     ]
     partial = pl.pallas_call(
-        functools.partial(attend_kernel, rope_width),
+        functools.partial(attend_kernel, rope_width, sp_count),
         out_shape=jax.ShapeDtypeStruct((tokens, model), low),
         in_specs=[VM] * 9,
         out_specs=VM,
         scratch_shapes=scratch,
-        compiler_params=pltpu.CompilerParams(vmem_limit_bytes=56 * 1024 * 1024),
+        compiler_params=pltpu.CompilerParams(
+            collective_id=0, has_side_effects=True, vmem_limit_bytes=48 * 1024 * 1024
+        ),
     )(
-        gathered,
+        own_latent,
         queries.reshape(tokens, width),
         query_rope.reshape(tokens, copies * rope_width),
         cosine,
@@ -515,18 +660,10 @@
     outgoing = jnp.concatenate([outgoing.reshape(sp_count, slots, model), extra], axis=2)
     arrived = swap_sp(outgoing, sp_count, 2)
     rows = sp_count * slots
-    everyone = gather_tp(arrived.reshape(rows, model + 128), tp_count, 3)
-    everyone = everyone.reshape(tp_count * rows, model + 128)
-    inputs = everyone[:, :model]
-    tail = everyone[:, model : model + 2 * experts_dev].astype(jnp.float32)
-    scale = tail[:, :experts_dev] + tail[:, experts_dev:]
-    gate_out = jnp.einsum("rd,edf->erf", inputs, gate_weight, preferred_element_type=jnp.float32)
-    up_out = jnp.einsum("rd,edf->erf", inputs, up_weight, preferred_element_type=jnp.float32)
-    hidden = (jax.nn.silu(gate_out) * up_out * scale.T[:, :, None]).astype(low)
-    expert_part = jnp.einsum(
-        "erf,efd->rd", hidden, down_weight, preferred_element_type=jnp.float32
-    ).astype(low)
-    expert_out = reduce_tp(expert_part.reshape(tp_count, rows, model), tp_count, 4).astype(low)
+    expert_part = experts_over_tp(
+        arrived.reshape(rows, model + 128), gate_weight, up_weight, down_weight, tp_count, 3
+    )
+    expert_out = reduce_tp(expert_part, tp_count, 4).astype(low)
     returned = swap_sp(expert_out.reshape(sp_count, slots, model), sp_count, 5)
     expert_mix = jnp.dot(
         pick_matrix.T, returned.reshape(rows, model), preferred_element_type=jnp.float32

time: 170 us -> 130 us (0.76)
  the two profiles are of different devices: /device:TPU:16 before, /device:TPU:0 now
where the time goes in v2:
time: 130 us
  Pallas kernels  116 us (89%)
  local copies, waits for them, and re-layouts  6.79 us (5%)
  other arithmetic  4.73 us (4%)
  matrix products  2.38 us (2%)
    pallas_call x4, Pallas kernels, comm_call(): pl.pallas_call(kernel, out_shape=out_shape, in_specs=[VM] * len(args), ou...  73.4 us
    pallas_call x1, Pallas kernels, experts_over_tp(): pl.pallas_call(functools.partial(expert_kernel, tp_count), out_shape=jax....  27.6 us
    pallas_call x1, Pallas kernels, local(): pl.pallas_call(functools.partial(attend_kernel, rope_width, sp_count), ou...  14.6 us
    unnamed x13, local copies, waits for them, and re-layouts  3.33 us

profile of v2, /device:TPU:0, one launch (start us, length us, event | category | flops | bytes accessed | tf_op | source)
XLA Modules:
  0.0 129.9 jit_solution(4464528289593882457)
XLA Ops:
  0.0 0.8 reduce_sum.47
  0.9 0.7 multiply_divide_fusion
  1.7 0.1 copy.87
  2.0 0.1 select_reduce_fusion
  2.1 0.3 copy.92
  2.4 0.1 copy.91
  2.5 0.1 copy.93
  2.6 0.1 copy.94
  2.9 0.2 multiply_cosine_fusion
  3.1 0.1 copy.83.sin_ref
  3.2 0.8 tile.12
  4.0 0.1 copy.81.cos_ref
  4.1 0.1 copy.80
  4.3 0.2 fusion.4
  4.5 1.2 fusion.5
  5.7 1.2 fusion.7
  6.9 1.1 copy.96
  8.0 1.0 copy.84.qr_ref
  9.0 1.1 copy.97
  10.1 1.1 copy.98
  11.3 14.6 %shard_map.154 = bf16[384,2048]{1,0:T(8,128)(2,1)S(1)} custom-call(bf16[384,640]{1,0:T(8,128)(2,1)S(1)} %pad_maximum_fusion.x_ref, bf16[384,512]{1,0:T(8,128)(2,1)S(1)} %bitcast.41, bf16[384,128]{1,0:T(8,128)(2,1)S(1)} %copy.84.qr_ref, f32[384,128]{1,0:T(8,128)S(1)} %copy.81.cos_ref, f32[384,128]{1,0:T(8,128)S(1)} %copy.83.sin_ref, ...), custom_call_target="tpu_custom_call" | custom-call | tf_op jit(solution)/shard_map/pallas_call | solution.py:605
  25.9 21.4 %shard_map.155 = f32[48,2048]{1,0:T(8,128)S(1)} custom-call(bf16[8,48,2048]{2,1,0:T(8,128)(2,1)S(1)} %bitcast.37), custom_call_target="tpu_custom_call" | custom-call | tf_op jit(solution)/shard_map/pallas_call | solution.py:52
  47.4 0.2 multiply_reduce_fusion
  47.7 1.2 convolution_convert_fusion
  49.0 0.1 reshape.169
  49.1 18.0 %shard_map.156 = bf16[4,18,2176]{2,1,0:T(8,128)(2,1)S(1)} custom-call(bf16[4,18,2176]{2,1,0:T(8,128)(2,1)S(1)} %pad_maximum_fusion.1.x_ref), custom_call_target="tpu_custom_call" | custom-call | tf_op jit(solution)/shard_map/pallas_call | solution.py:52
  67.1 0.1 reshape.171.x_ref
  67.2 27.6 %shard_map.157.x_ref = bf16[8,72,2048]{2,1,0:T(8,128)(2,1)S(1)} custom-call(bf16[72,2176]{1,0:T(8,128)(2,1)S(1)} %reshape.171.x_ref, bf16[2,2048,512]{2,1,0:T(8,128)(2,1)} %gate_ref.1, bf16[2,2048,512]{2,1,0:T(8,128)(2,1)} %up_ref.1, bf16[2,512,2048]{2,1,0:T(8,128)(2,1)} %down_ref.1), custom_call_target="tpu_custom_call" | custom-call | tf_op jit(solution)/shard_map/pallas_call | solution.py:216
  94.8 27.2 %shard_map.158 = f32[72,2048]{1,0:T(8,128)S(1)} custom-call(bf16[8,72,2048]{2,1,0:T(8,128)(2,1)S(1)} %shard_map.157.x_ref), custom_call_target="tpu_custom_call" | custom-call | tf_op jit(solution)/shard_map/pallas_call | solution.py:52
  122.1 0.1 reshape.172.x_ref
  122.2 6.7 %shard_map.159 = bf16[4,18,2048]{2,1,0:T(8,128)(2,1)S(1)} custom-call(bf16[4,18,2048]{2,1,0:T(8,128)(2,1)S(1)} %reshape.172.x_ref), custom_call_target="tpu_custom_call" | custom-call | tf_op jit(solution)/shard_map/pallas_call | solution.py:52
  128.9 0.9 fusion.1
  (42 shorter events, 0.8 us)
Async XLA Ops:
  0.0 1.5 %copy-start = (s32[384,2]{0,1:T(2,128)S(1)}, s32[384,2]{0,1:T(2,128)}, u32[]{:S(2)}) copy-start(s32[384,2]{0,1:T(2,128)} %param.26) | copy-start | bytes 9220
  0.0 11.3 %copy-start.1 = (bf16[2,256,2048]{2,1,0:T(8,128)(2,1)S(1)}, bf16[2,256,2048]{2,1,0:T(8,128)(2,1)}, u32[]{:S(2)}) copy-start(bf16[2,256,2048]{2,1,0:T(8,128)(2,1)} %param.24) | copy-start | bytes 6291460
  11.3 36.1 %copy-start.2 = (bf16[48,2048]{1,0:T(8,128)(2,1)S(1)}, bf16[48,2048]{1,0:T(8,128)(2,1)}, u32[]{:S(2)}) copy-start(bf16[48,2048]{1,0:T(8,128)(2,1)} %param.16) | copy-start | bytes 589828
  11.3 36.5 %copy-start.4 = (f32[2048]{0:T(1024)S(1)}, f32[2048]{0:T(1024)}, u32[]{:S(2)}) copy-start(f32[2048]{0:T(1024)} %param.25) | copy-start | bytes 24580
  94.8 34.1 %copy-start.3 = (bf16[48,2048]{1,0:T(8,128)(2,1)S(1)}, bf16[48,2048]{1,0:T(8,128)(2,1)}, u32[]{:S(2)}) copy-start(bf16[48,2048]{1,0:T(8,128)(2,1)} %param.16) | copy-start | bytes 589828

commit v3 on v2

--- a/solution.py
+++ b/solution.py
@@ -18,8 +18,9 @@
 VM = pl.BlockSpec(memory_space=pltpu.VMEM)
 
 
-def angle_tables(places, rope_width):
-    frequencies = rope_base ** (-jnp.arange(0, rope_width, 2, dtype=jnp.float32) / rope_width)
+def angle_tables(places, rope_width, repeats):
+    steps = jnp.arange(repeats * rope_width // 2, dtype=jnp.int32) % (rope_width // 2)
+    frequencies = rope_base ** (-(2 * steps).astype(jnp.float32) / rope_width)
     angles = places[:, None] * frequencies[None, :]
     return (jnp.cos(angles), jnp.sin(angles))
 
@@ -106,6 +107,8 @@
     experts = gate_ref.shape[0]
     model = gate_ref.shape[1]
     rows = x_ref.shape[0]
+    middle = x_ref.shape[1] // 256 * 128
+    parts = (slice(0, middle), slice(middle, x_ref.shape[1]))
     loads = [
         pltpu.make_async_copy(source, target, wsem.at[i])
         for i, (source, target) in enumerate(((gate_ref, gate), (up_ref, up), (down_ref, down)))
@@ -114,48 +117,58 @@
         load.start()
     greet_some([(True, partner), (has_above, above), (has_below, below)])
 
-    def move(block, sem, target, source=None):
+    def move(block, sems, place, part, target, source=None):
         source = held.at[block] if source is None else source
-        return remote(source, held.at[block], sem, recv.at[block], target)
-
-    @pl.when(has_above)
-    def _():
-        move(tp, usend.at[z], above, x_ref).start()
-
-    @pl.when(has_below)
-    def _():
-        move(tp, dsend.at[z], below, x_ref).start()
-
-    move(tp, psend.at[z], partner, x_ref).start()
+        return remote(
+            source.at[:, parts[part]],
+            held.at[block, :, parts[part]],
+            sems.at[place, part],
+            recv.at[block, part],
+            target,
+        )
+
+    for part in range(2):
+
+        @pl.when(has_above)
+        def _():
+            move(tp, usend, z, part, above, x_ref).start()
+
+        @pl.when(has_below)
+        def _():
+            move(tp, dsend, z, part, below, x_ref).start()
+
+        move(tp, psend, z, part, partner, x_ref).start()
     held[tp] = x_ref[...]
 
     def take(k):
         low, high = z - k, z + k
-
-        @pl.when(low >= 0)
-        def _():
-            block = low * 2 + core
-            move(block, usend.at[low], partner).wait_recv()
-
-            @pl.when(has_above)
+        for part in range(2):
+
+            @pl.when(low >= 0)
             def _():
-                move(block, usend.at[low], above).start()
-
-            move(block, psend.at[low], partner).start()
-
-        @pl.when(high < depth)
-        def _():
-            block = high * 2 + core
-            move(block, dsend.at[high], partner).wait_recv()
-
-            @pl.when(has_below)
+                block = low * 2 + core
+                move(block, usend, low, part, partner).wait_recv()
+
+                @pl.when(has_above)
+                def _():
+                    move(block, usend, low, part, above).start()
+
+                move(block, psend, low, part, partner).start()
+
+            @pl.when(high < depth)
             def _():
-                move(block, dsend.at[high], below).start()
-
-            move(block, psend.at[high], partner).start()
+                block = high * 2 + core
+                move(block, dsend, high, part, partner).wait_recv()
+
+                @pl.when(has_below)
+                def _():
+                    move(block, dsend, high, part, below).start()
+
+                move(block, psend, high, part, partner).start()
 
     def compute(place):
-        move(place * 2 + 1 - core, psend.at[place], partner).wait_recv()
+        for part in range(2):
+            move(place * 2 + 1 - core, psend, place, part, partner).wait_recv()
         blocks = pl.ds(place * 2, 2)
         x = held[blocks].reshape(2 * rows, held.shape[2])
         inputs = x[:, :model]
@@ -196,16 +209,17 @@
 
     lax.fori_loop(0, depth, step, 0)
     for place in range(depth):
-
-        @pl.when(has_above & (place <= z))
-        def _():
-            move(place * 2 + core, usend.at[place], above).wait_send()
-
-        @pl.when(has_below & (place >= z))
-        def _():
-            move(place * 2 + core, dsend.at[place], below).wait_send()
-
-        move(place * 2 + core, psend.at[place], partner).wait_send()
+        for part in range(2):
+
+            @pl.when(has_above & (place <= z))
+            def _():
+                move(place * 2 + core, usend, place, part, above).wait_send()
+
+            @pl.when(has_below & (place >= z))
+            def _():
+                move(place * 2 + core, dsend, place, part, below).wait_send()
+
+            move(place * 2 + core, psend, place, part, partner).wait_send()
 
 
 def experts_over_tp(x, gate_weight, up_weight, down_weight, tp_count, identity):
@@ -223,10 +237,10 @@
             pltpu.VMEM(gate_weight.shape, gate_weight.dtype),
             pltpu.VMEM(up_weight.shape, up_weight.dtype),
             pltpu.VMEM(down_weight.shape, down_weight.dtype),
-            dma((depth,)),
-            dma((depth,)),
-            dma((depth,)),
-            dma((tp_count,)),
+            dma((depth, 2)),
+            dma((depth, 2)),
+            dma((depth, 2)),
+            dma((tp_count, 2)),
             dma((3,)),
         ],
         compiler_params=pltpu.CompilerParams(
@@ -241,87 +255,104 @@
     sp, core, z, depth, partner, above, below, has_above, has_below = line(tp_count)
     greet_some([(True, partner), (has_above, above), (has_below, below)])
 
-    def swap(place):
+    middle = x_ref.shape[2] // 256 * 128
+    parts = (slice(0, middle), slice(middle, x_ref.shape[2]))
+
+    def swap(place, part):
         return remote(
-            x_ref.at[place * 2 + 1 - core],
-            partner_in.at[place],
-            send.at[place],
-            recv.at[place],
+            x_ref.at[place * 2 + 1 - core, :, parts[part]],
+            partner_in.at[place, :, parts[part]],
+            send.at[place, part],
+            recv.at[place, part],
             partner,
         )
 
-    def up(place):
+    def pass_on(place, part, arrivals, sems, target):
         return remote(
-            stage.at[place], up_in.at[place], zsend.at[place], urecv.at[place], above
-        )
-
-    def down(place):
-        return remote(
-            stage.at[place], down_in.at[place], zsend.at[place], drecv.at[place], below
-        )
-
-    def pair_sum(place):
-        swap(place).wait_recv()
-        return x_ref[place * 2 + core].astype(jnp.float32) + partner_in[place].astype(jnp.float32)
+            stage.at[place, :, parts[part]],
+            arrivals.at[place, :, parts[part]],
+            zsend.at[place, part],
+            sems.at[place, part],
+            target,
+        )
+
+    def up(place, part):
+        return pass_on(place, part, up_in, urecv, above)
+
+    def down(place, part):
+        return pass_on(place, part, down_in, drecv, below)
+
+    def pair_sum(place, part):
+        swap(place, part).wait_recv()
+        mine = x_ref[place * 2 + core, :, parts[part]].astype(jnp.float32)
+        return mine + partner_in[place, :, parts[part]].astype(jnp.float32)
 
     for j in range(depth):
-        swap(depth - 1 - j).start()
-        if depth - 1 - j > j:
-            swap(j).start()
+        for part in range(2):
+            swap(depth - 1 - j, part).start()
+            if depth - 1 - j > j:
+                swap(j, part).start()
         if depth - 1 - j <= j + 1:
             break
 
     for j in range(depth - 1):
         high, low = depth - 1 + z - j, j + z + 1 - depth
-
-        @pl.when(z <= j)
-        def _():
-            stage[high] = pair_sum(high).astype(stage.dtype)
-
-            @pl.when(has_below)
+        for part in range(2):
+            span = parts[part]
+
+            @pl.when(z <= j)
             def _():
-                up(high).wait_recv()
-                stage[high] = (
-                    stage[high].astype(jnp.float32) + up_in[high].astype(jnp.float32)
-                ).astype(stage.dtype)
-
-            up(high).start()
-
-        @pl.when(low >= 0)
-        def _():
-            stage[low] = pair_sum(low).astype(stage.dtype)
-
-            @pl.when(has_above)
+                stage[high, :, span] = pair_sum(high, part).astype(stage.dtype)
+
+                @pl.when(has_below)
+                def _():
+                    up(high, part).wait_recv()
+                    stage[high, :, span] = (
+                        stage[high, :, span].astype(jnp.float32)
+                        + up_in[high, :, span].astype(jnp.float32)
+                    ).astype(stage.dtype)
+
+                up(high, part).start()
+
+            @pl.when(low >= 0)
             def _():
-                down(low).wait_recv()
-                stage[low] = (
-                    stage[low].astype(jnp.float32) + down_in[low].astype(jnp.float32)
-                ).astype(stage.dtype)
-
-            down(low).start()
-
-    out_ref[...] = pair_sum(z)
-
-    @pl.when(has_below)
-    def _():
-        up(z).wait_recv()
-        out_ref[...] += up_in[z].astype(jnp.float32)
-
-    @pl.when(has_above)
-    def _():
-        down(z).wait_recv()
-        out_ref[...] += down_in[z].astype(jnp.float32)
+                stage[low, :, span] = pair_sum(low, part).astype(stage.dtype)
+
+                @pl.when(has_above)
+                def _():
+                    down(low, part).wait_recv()
+                    stage[low, :, span] = (
+                        stage[low, :, span].astype(jnp.float32)
+                        + down_in[low, :, span].astype(jnp.float32)
+                    ).astype(stage.dtype)
+
+                down(low, part).start()
+
+    for part in range(2):
+        span = parts[part]
+        out_ref[:, span] = pair_sum(z, part)
+
+        @pl.when(has_below)
+        def _():
+            up(z, part).wait_recv()
+            out_ref[:, span] += up_in[z, :, span].astype(jnp.float32)
+
+        @pl.when(has_above)
+        def _():
+            down(z, part).wait_recv()
+            out_ref[:, span] += down_in[z, :, span].astype(jnp.float32)
 
     for place in range(depth):
-        swap(place).wait_send()
-
-        @pl.when(place > z)
-        def _():
-            up(place).wait_send()
-
-        @pl.when(place < z)
-        def _():
-            down(place).wait_send()
+        for part in range(2):
+            swap(place, part).wait_send()
+
+            @pl.when(place > z)
+            def _():
+                up(place, part).wait_send()
+
+            @pl.when(place < z)
+            def _():
+                down(place, part).wait_send()
 
 
 def reduce_tp(x, tp_count, identity):
@@ -331,7 +362,7 @@
     return comm_call(
         functools.partial(reduce_tp_kernel, tp_count),
         jax.ShapeDtypeStruct(block, jnp.float32),
-        [buffer] * 4 + [pltpu.SemaphoreType.DMA((depth,))] * 5,
+        [buffer] * 4 + [pltpu.SemaphoreType.DMA((depth, 2))] * 5,
         identity,
         (x,),
     )
@@ -574,9 +605,7 @@
 
     first_place = lax.axis_index("sp") * tokens
     places = (first_place + jnp.arange(tokens, dtype=jnp.int32)).astype(jnp.float32)
-    cosine, sine = angle_tables(places, rope_width)
-    cosine = jnp.tile(cosine, (1, 2 * copies))
-    sine = jnp.tile(sine, (1, 2 * copies))
+    cosine, sine = angle_tables(places, rope_width, 2 * copies)
     index = jnp.arange(copies * rope_width, dtype=jnp.int32)
     source = jnp.where(index % rope_width < half, index + half, index - half)
     sign = jnp.where(index % rope_width < half, -1.0, 1.0)

time: 130 us -> 122 us (0.938)
  Pallas kernels: 116 us -> 108 us
    pallas_call x4, Pallas kernels: 73.4 us -> 66.8 us  [comm_call(): pl.pallas_call(kernel, out_shape=out_shape, in_specs=[VM] * len(args), ou...]
where the time goes in v3:
time: 122 us; the launch traced here: 121 us
  Pallas kernels  108 us (89%)
  local copies, waits for them, and re-layouts  5.62 us (5%)
  other arithmetic  5.31 us (4%)
  matrix products  2.07 us (2%)
    pallas_call x4, Pallas kernels, comm_call(): pl.pallas_call(kernel, out_shape=out_shape, in_specs=[VM] * len(args), ou...  66.8 us
    pallas_call x1, Pallas kernels, experts_over_tp(): pl.pallas_call(functools.partial(expert_kernel, tp_count), out_shape=jax....  26.6 us
    pallas_call x1, Pallas kernels, local(): pl.pallas_call(functools.partial(attend_kernel, rope_width, sp_count), ou...  14.6 us
    unnamed x13, local copies, waits for them, and re-layouts  3.33 us

profile of v3, /device:TPU:0, one launch (start us, length us, event | category | flops | bytes accessed | tf_op | source)
XLA Modules:
  0.0 121.3 jit_solution(16425646856175885707)
XLA Ops:
  0.0 0.8 reduce_sum.47
  0.9 0.7 multiply_divide_fusion
  1.7 0.1 copy.67
  2.0 0.1 select_reduce_fusion
  2.1 0.3 copy.72
  2.4 0.1 copy.71
  2.5 0.1 copy.73
  2.6 0.1 copy.74
  2.8 0.1 fusion.15
  2.9 0.7 tile.4
  3.6 0.1 copy.64
  3.8 0.8 fusion.4
  4.6 1.2 fusion.5
  5.8 1.2 fusion.7
  7.0 1.1 copy.76
  8.1 0.1 copy.66.qr_ref
  8.2 0.8 multiply_sine_fusion
  9.0 1.1 copy.77
  10.1 1.1 copy.78
  11.3 14.6 %shard_map.154 = bf16[384,2048]{1,0:T(8,128)(2,1)S(1)} custom-call(bf16[384,640]{1,0:T(8,128)(2,1)S(1)} %pad_maximum_fusion.x_ref, bf16[384,512]{1,0:T(8,128)(2,1)S(1)} %bitcast.39, bf16[384,128]{1,0:T(8,128)(2,1)S(1)} %copy.66.qr_ref, f32[384,128]{1,0:T(8,128)S(1)} %get-tuple-element.6.cos_ref, f32[384,128]{1,0:T(8,128)S(1)} %get-tuple-element.5.sin_ref, ...), custom_call_target="tpu_custom_call" | custom-call | tf_op jit(solution)/shard_map/pallas_call | solution.py:634
  26.0 17.8 %shard_map.155 = f32[48,2048]{1,0:T(8,128)S(1)} custom-call(bf16[8,48,2048]{2,1,0:T(8,128)(2,1)S(1)} %bitcast.35), custom_call_target="tpu_custom_call" | custom-call | tf_op jit(solution)/shard_map/pallas_call | solution.py:53
  43.8 0.2 multiply_reduce_fusion
  44.0 0.1 eq.75
  44.1 0.3 convolution_convert_fusion
  44.4 0.1 reshape.117
  44.6 18.5 %shard_map.156 = bf16[4,18,2176]{2,1,0:T(8,128)(2,1)S(1)} custom-call(bf16[4,18,2176]{2,1,0:T(8,128)(2,1)S(1)} %pad_maximum_fusion.1.x_ref), custom_call_target="tpu_custom_call" | custom-call | tf_op jit(solution)/shard_map/pallas_call | solution.py:53
  63.0 0.1 reshape.119.x_ref
  63.1 26.6 %shard_map.157.x_ref = bf16[8,72,2048]{2,1,0:T(8,128)(2,1)S(1)} custom-call(bf16[72,2176]{1,0:T(8,128)(2,1)S(1)} %reshape.119.x_ref, bf16[2,2048,512]{2,1,0:T(8,128)(2,1)} %gate_ref.1, bf16[2,2048,512]{2,1,0:T(8,128)(2,1)} %up_ref.1, bf16[2,512,2048]{2,1,0:T(8,128)(2,1)} %down_ref.1), custom_call_target="tpu_custom_call" | custom-call | tf_op jit(solution)/shard_map/pallas_call | solution.py:230
  89.7 22.7 %shard_map.158 = f32[72,2048]{1,0:T(8,128)S(1)} custom-call(bf16[8,72,2048]{2,1,0:T(8,128)(2,1)S(1)} %shard_map.157.x_ref), custom_call_target="tpu_custom_call" | custom-call | tf_op jit(solution)/shard_map/pallas_call | solution.py:53
  112.4 0.1 reshape.120.x_ref
  112.5 7.8 %shard_map.159 = bf16[4,18,2048]{2,1,0:T(8,128)(2,1)S(1)} custom-call(bf16[4,18,2048]{2,1,0:T(8,128)(2,1)S(1)} %reshape.120.x_ref), custom_call_target="tpu_custom_call" | custom-call | tf_op jit(solution)/shard_map/pallas_call | solution.py:53
  120.4 0.9 fusion.1
  (38 shorter events, 0.6 us)
Async XLA Ops:
  0.0 1.5 %copy-start = (s32[384,2]{0,1:T(2,128)S(1)}, s32[384,2]{0,1:T(2,128)}, u32[]{:S(2)}) copy-start(s32[384,2]{0,1:T(2,128)} %param.26) | copy-start | bytes 9220
  0.0 8.1 %copy-start.3 = (bf16[384,2,64]{0,2,1:T(8,128)(2,1)S(1)}, bf16[384,2,64]{0,2,1:T(8,128)(2,1)}, u32[]{:S(2)}) copy-start(bf16[384,2,64]{0,2,1:T(8,128)(2,1)} %param.18) | copy-start | bytes 294916
  0.0 11.3 %copy-start.1 = (bf16[2,256,2048]{2,1,0:T(8,128)(2,1)S(1)}, bf16[2,256,2048]{2,1,0:T(8,128)(2,1)}, u32[]{:S(2)}) copy-start(bf16[2,256,2048]{2,1,0:T(8,128)(2,1)} %param.24) | copy-start | bytes 6291460
  11.3 32.5 %copy-start.2 = (bf16[48,2048]{1,0:T(8,128)(2,1)S(1)}, bf16[48,2048]{1,0:T(8,128)(2,1)}, u32[]{:S(2)}) copy-start(bf16[48,2048]{1,0:T(8,128)(2,1)} %param.16) | copy-start | bytes 589828
  11.3 32.8 %copy-start.4 = (f32[2048]{0:T(1024)S(1)}, f32[2048]{0:T(1024)}, u32[]{:S(2)}) copy-start(f32[2048]{0:T(1024)} %param.25) | copy-start | bytes 24580
